TPU v7x, 256 devices: a whole 4x4x8 slice. The times are simulated.
256 devices in a mesh: kv: 32 (over z, y), tp: 8 (over x, core).
Axes of the slice: x: 4, y: 4, z: 8, core: 2. Of those that a mesh axis runs over, the one named last changes fastest.
Arguments:
- residual_in: bfloat16 [256, 2048], P(None, ('kv', 'tp')), may hold values from -14 to 14
- delta_state: float32 [256, 32, 128, 128], P('kv', 'tp'), may hold values from -1 to 1
- norm_gain_first: float32 [2048], P('kv'), may hold values from 0.1 to 1.9
- gate_first: bfloat16 [2048, 5632], P('kv', 'tp'), may hold values from -0.125 to 0.125
- up_first: bfloat16 [2048, 5632], P('kv', 'tp'), may hold values from -0.125 to 0.125
- down_first: bfloat16 [5632, 2048], P('tp', 'kv'), may hold values from -0.15625 to 0.15625
- norm_gain_mixer: float32 [2048], P('kv'), may hold values from 0.1 to 1.9
- query_weight: bfloat16 [2048, 2048], P('kv', 'tp'), may hold values from -0.125 to 0.125
- key_weight: bfloat16 [2048, 2048], P('kv', 'tp'), may hold values from -0.125 to 0.125
- value_weight: bfloat16 [2048, 4096], P('kv', 'tp'), may hold values from -0.125 to 0.125
- output_gate_weight: bfloat16 [2048, 4096], P('kv', 'tp'), may hold values from -0.125 to 0.125
- beta_weight: bfloat16 [2048, 32], P('kv'), may hold values from -0.125 to 0.125
- decay_weight: bfloat16 [2048, 32], P('kv'), may hold values from -0.125 to 0.125
- decay_rate: float32 [32], P('tp'), may hold values from -2.3 to 1.1
- decay_bias: float32 [32], P('tp'), may hold values from -1 to 1
- head_gain: float32 [128], replicated, may hold values from 0.1 to 1.9
- out_weight: bfloat16 [4096, 2048], P('tp', 'kv'), may hold values from -0.125 to 0.125
- norm_gain_second: float32 [2048], P('kv'), may hold values from 0.1 to 1.9
- gate_second: bfloat16 [2048, 5632], P('kv', 'tp'), may hold values from -0.125 to 0.125
- up_second: bfloat16 [2048, 5632], P('kv', 'tp'), may hold values from -0.125 to 0.125
- down_second: bfloat16 [5632, 2048], P('tp', 'kv'), may hold values from -0.15625 to 0.15625
Outputs:
- residual_out: bfloat16 [256, 2048], P(None, ('kv', 'tp'))
- delta_state_out: float32 [256, 32, 128, 128], P('kv', 'tp')
All inputs are finite; a program needn't handle non-finite values.
Results may differ from a plain program's by a relative error of at most 0.03.
Values may be sent and summed in bfloat16 or wider, within the bound.
No kernel may reach another device: no remote copies, remote signals or barrier semaphores. Data moves between devices by JAX's collectives and lax.ppermute only.
A program may use at most 64 MiB of HBM per device.

v0:
```python
import jax
import jax.numpy as jnp
from jax import lax
from jax.sharding import PartitionSpec as P

D = 2048


epsilon = 1e-06


def in_blocks(value, dim, size):
    before, after = (value.shape[:dim], value.shape[dim + 1 :])
    return jnp.moveaxis(value.reshape(*before, size, -1, *after), dim, 0)


def summed_on_arrival(value, axis, dim):
    blocks = in_blocks(value, dim, lax.axis_size(axis))
    arrived = lax.all_to_all(blocks, axis, split_axis=0, concat_axis=0, tiled=True)
    return arrived.astype(jnp.float32).sum(axis=0)


def side_by_side(arrays, axis, dim, along):
    columns = [a.reshape(*a.shape[:along], -1) for a in arrays]
    both = jnp.concatenate(columns, axis=along)
    result, at, outs = (summed_on_arrival(both, axis, dim), 0, [])
    for a, column in zip(arrays, columns):
        piece = result[..., at : at + column.shape[along]]
        outs.append(piece.reshape(*piece.shape[:along], *a.shape[along:]))
        at += column.shape[along]
    return tuple(outs)


def joined_along(blocks, dim):
    dims = list(blocks.shape[1:])
    dims[dim] *= blocks.shape[0]
    return jnp.moveaxis(blocks, 0, dim).reshape(dims)


def from_everyone(value, axis):
    copies = jnp.broadcast_to(value, (lax.axis_size(axis), *value.shape))
    return lax.all_to_all(copies, axis, split_axis=0, concat_axis=0, tiled=True)


def collect(value, axis, dim):
    return joined_along(from_everyone(value, axis), dim)


def activate(summed, square_sums, hidden_cols):
    rowscale = lax.rsqrt(square_sums / D + epsilon)[:, None]
    gate_act = summed[:, :hidden_cols] * rowscale
    up_act = summed[:, hidden_cols:] * rowscale
    return (jax.nn.silu(gate_act) * up_act).astype(jnp.bfloat16)


def feed_forward(residual, norm_gain, gate_weight, up_weight, down_weight, finish):
    as_float = residual.astype(jnp.float32)
    squares = jnp.sum(as_float * as_float, axis=1)
    scaled = (as_float * norm_gain).astype(jnp.bfloat16)
    joined = jnp.concatenate([gate_weight, up_weight], axis=1)
    partial_value = jnp.dot(scaled, joined, preferred_element_type=jnp.float32)
    hidden_cols = gate_weight.shape[1]
    summed, square_sums = side_by_side(
        (partial_value.astype(jnp.bfloat16), squares.astype(jnp.bfloat16)), "kv", 0, 1
    )
    hidden = activate(summed, square_sums, hidden_cols)
    projected = jnp.dot(
        collect(hidden, "kv", 0), down_weight, preferred_element_type=jnp.float32
    ).astype(jnp.bfloat16)
    if finish:
        col_count = residual.shape[1] // lax.axis_size("tp")
        own_cols = lax.dynamic_slice_in_dim(
            as_float, lax.axis_index("tp") * col_count, col_count, 1
        )
        branch = summed_on_arrival(projected, "tp", 1)
        return (own_cols + 0.5 * branch).astype(jnp.bfloat16)
    branch = lax.psum(projected, "tp").astype(jnp.float32)
    return (as_float + 0.5 * branch).astype(jnp.bfloat16)


def unit_heads(projected, head_size):
    activated = jax.nn.silu(projected).reshape(projected.shape[0], -1, head_size)
    return activated * lax.rsqrt(jnp.sum(activated * activated, axis=-1, keepdims=True) + epsilon)


def delta_step(old_state, key_rows, queries, values, beta_gate, decay_gate):
    faded_state = old_state * decay_gate[:, :, None, None]
    predicted = jnp.einsum("rhab,rha->rhb", faded_state, key_rows, precision=lax.Precision.HIGHEST)
    correction = beta_gate[:, :, None] * (values - predicted)
    updated = faded_state + key_rows[:, :, :, None] * correction[:, :, None, :]
    reading = jnp.einsum("rhab,rha->rhb", updated, queries, precision=lax.Precision.HIGHEST)
    return (updated, reading)


def token_mixer(
    residual,
    norm_gain,
    query_weight,
    key_weight,
    value_weight,
    output_gate_weight,
    beta_weight,
    decay_weight,
    decay_rate,
    decay_bias,
    head_gain,
    out_weight,
    old_state,
):
    as_float = residual.astype(jnp.float32)
    squares = jnp.sum(as_float * as_float, axis=1)
    scaled = (as_float * norm_gain).astype(jnp.bfloat16)
    joined = jnp.concatenate([query_weight, key_weight, value_weight, output_gate_weight], axis=1)
    partial_value = jnp.dot(scaled, joined, preferred_element_type=jnp.float32)
    heads_dev = decay_rate.shape[0]
    head_start = lax.axis_index("tp") * heads_dev
    gate_cols = jnp.concatenate(
        [
            lax.dynamic_slice_in_dim(beta_weight, head_start, heads_dev, 1),
            lax.dynamic_slice_in_dim(decay_weight, head_start, heads_dev, 1),
        ],
        axis=1,
    )
    gate_part = jnp.dot(scaled, gate_cols, preferred_element_type=jnp.float32)
    row_count = old_state.shape[0]
    summed, gate_summed, square_sums = side_by_side(
        (
            partial_value.astype(jnp.bfloat16),
            gate_part.astype(jnp.bfloat16),
            squares.astype(jnp.bfloat16),
        ),
        "kv",
        0,
        1,
    )
    rowscale = lax.rsqrt(square_sums / D + epsilon)[:, None]
    summed = summed * rowscale
    gate_summed = gate_summed * rowscale
    head_size = old_state.shape[2]
    key_cols = query_weight.shape[1]
    value_cols = value_weight.shape[1]
    repeat_count = heads_dev // (key_cols // head_size)
    queries = jnp.repeat(
        unit_heads(summed[:, :key_cols], head_size) * head_size ** (-0.5), repeat_count, axis=1
    )
    key_rows = jnp.repeat(
        unit_heads(summed[:, key_cols : 2 * key_cols], head_size), repeat_count, axis=1
    )
    values = jax.nn.silu(summed[:, 2 * key_cols : 2 * key_cols + value_cols]).reshape(
        row_count, heads_dev, head_size
    )
    out_gate = jax.nn.silu(summed[:, 2 * key_cols + value_cols :]).reshape(
        row_count, heads_dev, head_size
    )
    beta_gate = jax.nn.sigmoid(gate_summed[:, :heads_dev])
    decay_gate = jnp.exp(
        -jnp.exp(decay_rate)[None, :]
        * jax.nn.softplus(gate_summed[:, heads_dev:] + decay_bias[None, :])
    )
    new_state, reading = delta_step(old_state, key_rows, queries, values, beta_gate, decay_gate)
    normed = reading * lax.rsqrt(jnp.mean(reading * reading, axis=-1, keepdims=True) + epsilon)
    normed = (
        (normed * head_gain * out_gate)
        .reshape(row_count, heads_dev * head_size)
        .astype(jnp.bfloat16)
    )
    projected = jnp.dot(
        collect(normed, "kv", 0), out_weight, preferred_element_type=jnp.float32
    ).astype(jnp.bfloat16)
    branch = lax.psum(projected, "tp").astype(jnp.float32)
    return ((as_float + branch).astype(jnp.bfloat16), new_state)


def body(
    residual_in,
    delta_state,
    norm_gain_first,
    gate_first,
    up_first,
    down_first,
    norm_gain_mixer,
    query_weight,
    key_weight,
    value_weight,
    output_gate_weight,
    beta_weight,
    decay_weight,
    decay_rate,
    decay_bias,
    head_gain,
    out_weight,
    norm_gain_second,
    gate_second,
    up_second,
    down_second,
):
    columns = lax.all_gather(residual_in, "tp", axis=1, tiled=True)
    after_first = feed_forward(columns, norm_gain_first, gate_first, up_first, down_first, False)
    after_mixer, new_state = token_mixer(
        after_first,
        norm_gain_mixer,
        query_weight,
        key_weight,
        value_weight,
        output_gate_weight,
        beta_weight,
        decay_weight,
        decay_rate,
        decay_bias,
        head_gain,
        out_weight,
        delta_state,
    )
    residual_out = feed_forward(
        after_mixer, norm_gain_second, gate_second, up_second, down_second, True
    )
    return (residual_out, new_state)


def solution(mesh):
    placed = (
        P(None, ("kv", "tp")),
        P("kv", "tp", None, None),
        P("kv"),
        P("kv", "tp"),
        P("kv", "tp"),
        P("tp", "kv"),
        P("kv"),
        P("kv", "tp"),
        P("kv", "tp"),
        P("kv", "tp"),
        P("kv", "tp"),
        P("kv", None),
        P("kv", None),
        P("tp"),
        P("tp"),
        P(),
        P("tp", "kv"),
        P("kv"),
        P("kv", "tp"),
        P("kv", "tp"),
        P("tp", "kv"),
    )
    return jax.shard_map(
        body,
        mesh=mesh,
        in_specs=placed,
        out_specs=(P(None, ("kv", "tp")), P("kv", "tp", None, None)),
        check_vma=False,
    )
```

profile of v0, /device:TPU:1, one launch (start us, length us, event | category | flops | bytes accessed | tf_op | source)
XLA Modules:
  0.0 230.6 jit_solution(4892839816095156955)
XLA Ops:
  0.6 0.0 copy-start
  0.6 16.2 %all_gather.3 = bf16[256,64]{0,1:T(8,128)(2,1)S(1)} all-gather(bf16[256,8]{0,1:T(8,128)(2,1)} %param.21), channel_id=1, replica_groups=mesh['kv'=32,'tp'=8] {'tp'}, dimensions={1}, use_global_device_ids=true | all-gather | bytes 36864 | tf_op jit(solution)/shard_map/all_gather | solution.py:197
  16.9 0.2 convert_element_type.152
  17.1 1.4 fusion
  18.5 0.1 pad_maximum_fusion
  18.6 0.0 copy-start.11
  18.6 0.0 copy-start.6
  18.6 0.0 copy-start.7
  18.6 0.0 copy-start.9
  18.7 0.0 copy-start.10
  18.7 31.4 %all_to_all.35 = bf16[32,8,1409]{2,1,0:T(8,128)(2,1)S(1)} all-to-all(bf16[32,8,1409]{2,1,0:T(8,128)(2,1)S(1)} %pad_maximum_fusion), channel_id=1, replica_groups=mesh['kv'=32,'tp'=8] {'kv'}, dimensions={0} | all-to-all | bytes 1442816 | tf_op jit(solution)/shard_map/all_to_all | solution.py:19
  50.1 0.1 convert_reduce_fusion.2
  50.2 0.1 fusion.57
  50.3 0.1 fusion.36
  50.4 0.8 broadcast_in_dim.10
  51.2 5.6 %all-to-all-start.1 = ((bf16[32,8,704]{2,1,0:T(8,128)(2,1)}), bf16[32,8,704]{2,1,0:T(8,128)(2,1)S(1)}, u32[]{:S(2)}, u32[]{:S(2)}) async-start(bf16[32,8,704]{2,1,0:T(8,128)(2,1)} %broadcast_in_dim.10), calls=%async_computation.1 | async-start | bytes 786432 | tf_op jit(solution)/shard_map/all_to_all | solution.py:42
  56.8 0.7 constant_dynamic-slice_fusion
  57.5 12.1 %all-to-all-done.1 = bf16[32,8,704]{2,1,0:T(8,128)(2,1)S(1)} async-done(((bf16[32,8,704]{2,1,0:T(8,128)(2,1)}), bf16[32,8,704]{2,1,0:T(8,128)(2,1)S(1)}, u32[]{:S(2)}, u32[]{:S(2)}) %all-to-all-start.1) | async-done | bytes 360480 | tf_op jit(solution)/shard_map/all_to_all | solution.py:42
  69.6 0.2 convolution_convert_fusion.5
  69.8 23.5 %psum.14 = bf16[256,64]{0,1:T(8,128)(2,1)S(1)} all-reduce(bf16[256,64]{0,1:T(8,128)(2,1)S(1)} %convolution_convert_fusion.5), channel_id=1, replica_groups=mesh['kv'=32,'tp'=8] {'tp'}, use_global_device_ids=true, to_apply=%region_2.3 | all-reduce | flops 16384 | bytes 65536 | tf_op jit(solution)/shard_map/psum | solution.py:77
  93.4 0.2 convolution_convert_fusion.6
  93.6 0.1 copy.64
  93.7 0.2 convert_element_type.153
  94.0 0.0 copy-start.15
  94.0 0.5 fusion.1
  94.5 0.0 copy-start.14
  94.5 0.0 copy-start.1
  94.5 1.1 concatenate.39
  95.6 4.6 %all-to-all-start.2 = ((bf16[32,8,1545]{2,1,0:T(8,128)(2,1)}), bf16[32,8,1545]{2,1,0:T(8,128)(2,1)S(1)}, u32[]{:S(2)}, u32[]{:S(2)}) async-start(bf16[32,8,1545]{2,1,0:T(8,128)(2,1)} %concatenate.39), calls=%async_computation.2 | async-start | bytes 1703936 | tf_op jit(solution)/shard_map/all_to_all | solution.py:19
  100.3 19.5 %all-to-all-done.2 = bf16[32,8,1545]{2,1,0:T(8,128)(2,1)S(1)} async-done(((bf16[32,8,1545]{2,1,0:T(8,128)(2,1)}), bf16[32,8,1545]{2,1,0:T(8,128)(2,1)S(1)}, u32[]{:S(2)}, u32[]{:S(2)}) %all-to-all-start.2) | async-done | bytes 791072 | tf_op jit(solution)/shard_map/all_to_all | solution.py:19
  119.7 0.1 convert_reduce_fusion
  119.8 0.2 fusion.54
  120.0 0.1 slice_multiply_fusion.7
  120.1 0.1 slice_multiply_fusion
  120.2 0.1 fusion.43
  120.3 0.1 add_divide_fusion
  120.4 0.1 copy.56
  120.5 0.1 fusion.44
  120.6 2.0 fusion.3
  122.6 0.1 fusion.40
  122.7 0.7 multiply_add_fusion
  123.5 0.0 copy-start.2
  123.5 0.0 copy-start.13
  123.5 0.0 copy-start.3
  123.5 0.0 copy-start.4
  123.6 1.2 copy-done.2
  124.8 1.9 fusion.67
  126.7 0.1 fusion.38
  126.8 0.1 fusion.46
  126.9 17.3 %all_to_all.36 = bf16[32,8,512]{2,1,0:T(8,128)(2,1)S(1)} all-to-all(bf16[32,8,512]{2,1,0:T(8,128)(2,1)S(1)} %broadcast_in_dim.13), channel_id=1, replica_groups=mesh['kv'=32,'tp'=8] {'kv'}, dimensions={0} | all-to-all | bytes 524288 | tf_op jit(solution)/shard_map/all_to_all | solution.py:42
  144.2 0.2 convolution_convert_fusion.3
  144.4 26.0 %psum.15 = bf16[256,64]{0,1:T(8,128)(2,1)S(1)} all-reduce(bf16[256,64]{0,1:T(8,128)(2,1)S(1)} %convolution_convert_fusion.3), channel_id=1, replica_groups=mesh['kv'=32,'tp'=8] {'tp'}, use_global_device_ids=true, to_apply=%region_8.9 | all-reduce | flops 16384 | bytes 65536 | tf_op jit(solution)/shard_map/psum | solution.py:170
  170.4 0.2 convert_element_type.154
  170.7 0.5 fusion.2
  171.1 0.1 pad_maximum_fusion.1
  171.2 22.8 %all_to_all.37 = bf16[32,8,1409]{2,1,0:T(8,128)(2,1)S(1)} all-to-all(bf16[32,8,1409]{2,1,0:T(8,128)(2,1)S(1)} %pad_maximum_fusion.1), channel_id=1, replica_groups=mesh['kv'=32,'tp'=8] {'kv'}, dimensions={0} | all-to-all | bytes 1442816 | tf_op jit(solution)/shard_map/all_to_all | solution.py:19
  194.0 0.1 convert_reduce_fusion.1
  194.1 0.1 fusion.51
  194.2 0.1 fusion.34
  194.4 18.7 %all_to_all.38 = bf16[32,8,704]{2,1,0:T(8,128)(2,1)S(1)} all-to-all(bf16[32,8,704]{2,1,0:T(8,128)(2,1)S(1)} %broadcast_in_dim.14), channel_id=1, replica_groups=mesh['kv'=32,'tp'=8] {'kv'}, dimensions={0} | all-to-all | bytes 720896 | tf_op jit(solution)/shard_map/all_to_all | solution.py:42
  213.1 0.9 fusion.5
  214.0 11.3 %all-to-all-start.6 = ((bf16[8,256,8]{1,2,0:T(8,128)(2,1)}), bf16[8,256,8]{1,2,0:T(8,128)(2,1)S(1)}, u32[]{:S(2)}, u32[]{:S(2)}) async-start(bf16[8,256,8]{1,2,0:T(8,128)(2,1)} %fusion.5), calls=%async_computation.6 | async-start | bytes 65536 | tf_op jit(solution)/shard_map/all_to_all | solution.py:19
  225.2 4.7 %all-to-all-done.6 = bf16[8,256,8]{1,2,0:T(8,128)(2,1)S(1)} async-done(((bf16[8,256,8]{1,2,0:T(8,128)(2,1)}), bf16[8,256,8]{1,2,0:T(8,128)(2,1)S(1)}, u32[]{:S(2)}, u32[]{:S(2)}) %all-to-all-start.6) | async-done | bytes 32800 | tf_op jit(solution)/shard_map/all_to_all | solution.py:19
  230.0 0.6 add_convert_fusion
  (33 shorter events, 0.3 us)
Async XLA Ops:
  0.6 68.9 %copy-start = (bf16[704,64]{0,1:T(8,128)(2,1)S(1)}, bf16[704,64]{0,1:T(8,128)(2,1)}, u32[]{:S(2)}) copy-start(bf16[704,64]{0,1:T(8,128)(2,1)} %param.26) | copy-start | bytes 270340
  18.6 74.8 %copy-start.11 = (f32[64]{0:T(128)S(1)}, f32[64]{0:T(128)}, u32[]{:S(2)}) copy-start(f32[64]{0:T(128)} %param.27) | copy-start | bytes 772
  18.6 75.4 %copy-start.6 = (bf16[64,512]{1,0:T(8,128)(2,1)S(1)}, bf16[64,512]{1,0:T(8,128)(2,1)}, u32[]{:S(2)}) copy-start(bf16[64,512]{1,0:T(8,128)(2,1)} %param.31) | copy-start | bytes 196612
  18.6 75.4 %copy-start.7 = (bf16[64,512]{1,0:T(8,128)(2,1)S(1)}, bf16[64,512]{1,0:T(8,128)(2,1)}, u32[]{:S(2)}) copy-start(bf16[64,512]{1,0:T(8,128)(2,1)} %param.30) | copy-start | bytes 196612
  18.6 75.4 %copy-start.9 = (bf16[64,256]{1,0:T(8,128)(2,1)S(1)}, bf16[64,256]{1,0:T(8,128)(2,1)}, u32[]{:S(2)}) copy-start(bf16[64,256]{1,0:T(8,128)(2,1)} %param.29) | copy-start | bytes 98308
  18.7 75.4 %copy-start.10 = (bf16[64,256]{1,0:T(8,128)(2,1)S(1)}, bf16[64,256]{1,0:T(8,128)(2,1)}, u32[]{:S(2)}) copy-start(bf16[64,256]{1,0:T(8,128)(2,1)} %param.28) | copy-start | bytes 98308
  51.2 18.4 %all-to-all-start.1 = ((bf16[32,8,704]{2,1,0:T(8,128)(2,1)}), bf16[32,8,704]{2,1,0:T(8,128)(2,1)S(1)}, u32[]{:S(2)}, u32[]{:S(2)}) async-start(bf16[32,8,704]{2,1,0:T(8,128)(2,1)} %broadcast_in_dim.10), calls=%async_computation.1 | async-start | bytes 786432 | tf_op jit(solution)/shard_map/all_to_all | solution.py:42
  94.0 6.2 %copy-start.15 = (f32[4]{0:T(128)S(1)}, f32[4]{0:T(128)}, u32[]{:S(2)}) copy-start(f32[4]{0:T(128)} %param.34) | copy-start | bytes 52
  94.5 25.8 %copy-start.14 = (f32[4]{0:T(128)S(1)}, f32[4]{0:T(128)}, u32[]{:S(2)}) copy-start(f32[4]{0:T(128)} %param.35) | copy-start | bytes 52
  94.5 26.1 %copy-start.1 = (f32[8,4,128,128]{3,2,1,0:T(8,128)S(1)}, f32[8,4,128,128]{3,2,1,0:T(8,128)}, u32[]{:S(2)}) copy-start(f32[8,4,128,128]{3,2,1,0:T(8,128)} %param.22) | copy-start | bytes 6291460
  95.6 24.1 %all-to-all-start.2 = ((bf16[32,8,1545]{2,1,0:T(8,128)(2,1)}), bf16[32,8,1545]{2,1,0:T(8,128)(2,1)S(1)}, u32[]{:S(2)}, u32[]{:S(2)}) async-start(bf16[32,8,1545]{2,1,0:T(8,128)(2,1)} %concatenate.39), calls=%async_computation.2 | async-start | bytes 1703936 | tf_op jit(solution)/shard_map/all_to_all | solution.py:19
  123.5 1.3 copy-start.2
  123.5 3.3 %copy-start.13 = (f32[128]{0:T(128)S(1)}, f32[128]{0:T(128)}, u32[]{:S(2)}) copy-start(f32[128]{0:T(128)} %param.36) | copy-start | bytes 1540
  123.5 20.7 %copy-start.8 = (bf16[512,64]{0,1:T(8,128)(2,1)S(1)}, bf16[512,64]{0,1:T(8,128)(2,1)}, u32[]{:S(2)}) copy-start(bf16[512,64]{0,1:T(8,128)(2,1)} %param.37) | copy-start | bytes 196612
  123.5 47.1 %copy-start.3 = (bf16[64,704]{1,0:T(8,128)(2,1)S(1)}, bf16[64,704]{1,0:T(8,128)(2,1)}, u32[]{:S(2)}) copy-start(bf16[64,704]{1,0:T(8,128)(2,1)} %param.40) | copy-start | bytes 270340
  123.5 47.1 %copy-start.4 = (bf16[64,704]{1,0:T(8,128)(2,1)S(1)}, bf16[64,704]{1,0:T(8,128)(2,1)}, u32[]{:S(2)}) copy-start(bf16[64,704]{1,0:T(8,128)(2,1)} %param.39) | copy-start | bytes 270340
  123.5 47.1 %copy-start.12 = (f32[64]{0:T(128)S(1)}, f32[64]{0:T(128)}, u32[]{:S(2)}) copy-start(f32[64]{0:T(128)} %param.38) | copy-start | bytes 772
  171.2 41.9 %copy-start.5 = (bf16[704,64]{0,1:T(8,128)(2,1)S(1)}, bf16[704,64]{0,1:T(8,128)(2,1)}, u32[]{:S(2)}) copy-start(bf16[704,64]{0,1:T(8,128)(2,1)} %param.41) | copy-start | bytes 270340
  214.0 16.0 %all-to-all-start.6 = ((bf16[8,256,8]{1,2,0:T(8,128)(2,1)}), bf16[8,256,8]{1,2,0:T(8,128)(2,1)S(1)}, u32[]{:S(2)}, u32[]{:S(2)}) async-start(bf16[8,256,8]{1,2,0:T(8,128)(2,1)} %fusion.5), calls=%async_computation.6 | async-start | bytes 65536 | tf_op jit(solution)/shard_map/all_to_all | solution.py:19
where the time goes:
time: 231 us
  blocking collectives  156 us (68%)
  waiting for transfers between devices  36.3 us (16%)
  starting transfers between devices  21.5 us (9%)
  matrix products  7.71 us (3%)
  local copies, waits for them, and re-layouts  4.91 us (2%)
  other arithmetic  3.23 us (1%)
    all_to_all x2, blocking collectives, summed_on_arrival(): lax.all_to_all(blocks, axis, split_axis=0, concat_axis=0, tiled=True)  54.2 us
    all_to_all x2, blocking collectives, from_everyone(): return lax.all_to_all(copies, axis, split_axis=0, concat_axis=0, tiled=True)  36 us
    psum x1, blocking collectives, token_mixer(): branch = lax.psum(projected, 'tp').astype(jnp.float32)  26 us
    all_to_all x2, waiting for transfers between devices, summed_on_arrival(): lax.all_to_all(blocks, axis, split_axis=0, concat_axis=0, tiled=True)  24.2 us
    psum x1, blocking collectives, feed_forward(): branch = lax.psum(projected, 'tp').astype(jnp.float32)  23.5 us
    all_gather x1, blocking collectives, body(): columns = lax.all_gather(residual_in, 'tp', axis=1, tiled=True)  16.2 us
    all_to_all x2, starting transfers between devices, summed_on_arrival(): lax.all_to_all(blocks, axis, split_axis=0, concat_axis=0, tiled=True)  15.9 us
    all_to_all x1, waiting for transfers between devices, from_everyone(): return lax.all_to_all(copies, axis, split_axis=0, concat_axis=0, tiled=True)  12.1 us
  transfers between devices with their start and end apart: 3, of which 3 were waited for; matrix products, arithmetic and copies ran while one was open for 0% of the time, Pallas kernels for 0%

commit v1 on v0

v1 whole, which is shorter than its diff:
```python
import jax
import jax.numpy as jnp
from jax import lax
from jax.sharding import Mesh
from jax.sharding import PartitionSpec as P

D = 2048
HEAD = 128
GATES = 128

epsilon = 1e-06

TP = ("x", "c")
ACROSS = ("z", "x", "c")

bf16 = jnp.bfloat16
f32 = jnp.float32


def exchange(blocks, axis):
    return lax.all_to_all(blocks, axis, split_axis=0, concat_axis=0, tiled=True)


def from_everyone(value, axis):
    return exchange(jnp.broadcast_to(value, (lax.axis_size(axis), *value.shape)), axis)


def everyone_sum(value, axis):
    return from_everyone(value, axis).astype(f32).sum(axis=0)


def times_transposed(left, right_rows):
    return lax.dot_general(left, right_rows, (((1,), (1,)), ((), ())), preferred_element_type=f32)


def square_columns(as_float):
    squares = jnp.sum(as_float * as_float, axis=1, keepdims=True)
    high = squares.astype(bf16).astype(f32)
    lane = lax.broadcasted_iota(jnp.int32, (squares.shape[0], GATES), 1)
    return jnp.where(lane == 0, high, jnp.where(lane == 1, squares - high, 0.0))


def row_scale(first_two):
    return lax.rsqrt((first_two[:, :1] + first_two[:, 1:2]) / D + epsilon)


def hidden_units(residual, gate_up):
    partial_value = jnp.dot(residual, gate_up, preferred_element_type=f32)
    both = jnp.concatenate([partial_value, square_columns(residual.astype(f32))], axis=1).astype(bf16)
    summed = everyone_sum(both, "y")
    width = gate_up.shape[1]
    scale = row_scale(summed[:, width:])
    gate_act = summed[:, : width // 2] * scale
    up_act = summed[:, width // 2 : width] * scale
    return (jax.nn.silu(gate_act) * up_act).astype(bf16)


def unit_heads(projected, head_size):
    activated = jax.nn.silu(projected).reshape(projected.shape[0], -1, head_size)
    return activated * lax.rsqrt(jnp.sum(activated * activated, axis=-1, keepdims=True) + epsilon)


def delta_step(old_state, key_rows, queries, values, beta_gate, decay_gate):
    faded_state = old_state * decay_gate[:, :, None, None]
    predicted = jnp.einsum("rhab,rha->rhb", faded_state, key_rows, precision=lax.Precision.HIGHEST)
    correction = beta_gate[:, :, None] * (values - predicted)
    updated = faded_state + key_rows[:, :, :, None] * correction[:, :, None, :]
    reading = jnp.einsum("rhab,rha->rhb", updated, queries, precision=lax.Precision.HIGHEST)
    return (updated, reading)


def mixer_values(residual, mixer_in, decay_rate, decay_bias, head_gain, old_state):
    row_count, heads_dev, head_size = old_state.shape[:3]
    projected = jnp.dot(residual, mixer_in, preferred_element_type=f32)
    width = mixer_in.shape[1] - GATES
    squares = square_columns(residual.astype(f32))
    tail = projected[:, width:] + jnp.roll(squares, 2 * heads_dev, axis=1)
    both = jnp.concatenate([projected[:, :width], tail], axis=1).astype(bf16)
    blocks = both.reshape(-1, row_count, both.shape[1])
    summed = exchange(blocks, "y").astype(f32).sum(axis=0)
    tail = summed[:, width:]
    scale = row_scale(tail[:, 2 * heads_dev :])
    summed = summed[:, :width] * scale
    gates = tail * scale
    value_cols = heads_dev * head_size
    key_cols = (width - 2 * value_cols) // 2
    repeat_count = value_cols // key_cols
    queries = jnp.repeat(
        unit_heads(summed[:, :key_cols], head_size) * head_size ** (-0.5), repeat_count, axis=1
    )
    key_rows = jnp.repeat(unit_heads(summed[:, key_cols : 2 * key_cols], head_size), repeat_count, axis=1)
    values = jax.nn.silu(summed[:, 2 * key_cols : 2 * key_cols + value_cols]).reshape(
        row_count, heads_dev, head_size
    )
    out_gate = jax.nn.silu(summed[:, 2 * key_cols + value_cols :]).reshape(row_count, heads_dev, head_size)
    beta_gate = jax.nn.sigmoid(gates[:, :heads_dev])
    decay_gate = jnp.exp(
        -jnp.exp(decay_rate)[None, :]
        * jax.nn.softplus(gates[:, heads_dev : 2 * heads_dev] + decay_bias[None, :])
    )
    new_state, reading = delta_step(old_state, key_rows, queries, values, beta_gate, decay_gate)
    normed = reading * lax.rsqrt(jnp.mean(reading * reading, axis=-1, keepdims=True) + epsilon)
    normed = (normed * head_gain * out_gate).reshape(row_count, value_cols).astype(bf16)
    return normed, new_state


def body(
    residual_in,
    delta_state,
    norm_gain_first,
    gate_first,
    up_first,
    down_first,
    norm_gain_mixer,
    query_weight,
    key_weight,
    value_weight,
    output_gate_weight,
    beta_weight,
    decay_weight,
    decay_rate,
    decay_bias,
    head_gain,
    out_weight,
    norm_gain_second,
    gate_second,
    up_second,
    down_second,
):
    planes, tp_count = lax.axis_size("z"), lax.axis_size(TP)
    heads_dev = decay_rate.shape[0]

    def scaled_rows(gain, weights):
        return (jnp.concatenate(weights, axis=1).astype(f32) * gain[:, None]).astype(bf16)

    def gathered(weights):
        return lax.all_gather(jnp.concatenate(weights, axis=1), "z", axis=0, tiled=True)

    head_start = lax.axis_index(TP) * heads_dev
    gate_cols = [
        lax.dynamic_slice_in_dim(beta_weight, head_start, heads_dev, 1),
        lax.dynamic_slice_in_dim(decay_weight, head_start, heads_dev, 1),
        jnp.zeros((beta_weight.shape[0], GATES - 2 * heads_dev), bf16),
    ]
    first_in = scaled_rows(norm_gain_first, [gate_first, up_first])
    mixer_in = scaled_rows(
        norm_gain_mixer, [query_weight, key_weight, value_weight, output_gate_weight, *gate_cols]
    )
    second_in = scaled_rows(norm_gain_second, [gate_second, up_second])
    width, mixer_width = first_in.shape[1], mixer_in.shape[1]
    first_in = gathered([first_in])
    middle = gathered([down_first.T, mixer_in])
    last = gathered([out_weight.T, second_in, down_second.T])
    down_first, mixer_in = middle[:, : width // 2], middle[:, width // 2 :]
    values_width = out_weight.shape[0]
    out_rows, second_in, down_second = (
        last[:, :values_width],
        last[:, values_width : values_width + width],
        last[:, values_width + width :],
    )

    columns = residual_in.T
    own_cols, rows = columns.shape[0], columns.shape[1] // planes
    pieces = jnp.moveaxis(columns.reshape(own_cols, planes, rows), 1, 0)
    pieces = jnp.broadcast_to(pieces[:, None], (planes, tp_count, own_cols, rows))
    residual = exchange(pieces.reshape(-1, own_cols, rows), ACROSS).reshape(-1, rows).T

    hidden = hidden_units(residual, first_in)
    projected = times_transposed(hidden, down_first).astype(bf16)
    after_first = (residual.astype(f32) + 0.5 * everyone_sum(projected, TP)).astype(bf16)

    normed, new_state = mixer_values(
        after_first, mixer_in, decay_rate, decay_bias, head_gain, delta_state
    )
    normed = from_everyone(normed, "y").reshape(rows, -1)
    projected = times_transposed(normed, out_rows).astype(bf16)
    after_mixer = (after_first.astype(f32) + everyone_sum(projected, TP)).astype(bf16)

    hidden = hidden_units(after_mixer, second_in)
    projected = times_transposed(down_second, hidden).astype(bf16)
    pieces = jnp.concatenate([projected, after_mixer.T], axis=1)
    arrived = exchange(pieces.reshape(-1, own_cols, 2 * rows), ACROSS)
    arrived = arrived.reshape(planes, tp_count, own_cols, 2 * rows).astype(f32)
    final = arrived[:, 0, :, rows:] + 0.5 * arrived[..., :rows].sum(axis=1)
    residual_out = jnp.moveaxis(final, 1, 2).reshape(planes * rows, own_cols).astype(bf16)
    return (residual_out, new_state)


def solution(mesh):
    cut = Mesh(mesh.devices.reshape(8, 4, 4, 2), ("z", "y", "x", "c"))
    kv, tp = ("z", "y"), ("x", "c")
    wide, tall = P(kv, tp), P(tp, kv)
    placed = (
        P(None, kv + tp),
        P(kv, tp, None, None),
        P(kv),
        wide,
        wide,
        tall,
        P(kv),
        wide,
        wide,
        wide,
        wide,
        P(kv, None),
        P(kv, None),
        P(tp),
        P(tp),
        P(),
        tall,
        P(kv),
        wide,
        wide,
        tall,
    )
    return jax.shard_map(
        body,
        mesh=cut,
        in_specs=placed,
        out_specs=(P(None, kv + tp), P(kv, tp, None, None)),
        check_vma=False,
    )
```

time: 231 us -> 201 us (0.87)
  blocking collectives: 156 us -> 38.6 us
  waiting for transfers between devices: 36.3 us -> 82.7 us
  between operations: 1.06 us -> 14.1 us
  starting transfers between devices: 21.5 us -> 33.8 us
  matrix products: 7.71 us -> 13.8 us
  other arithmetic: 3.23 us -> 8.8 us
  local copies, waits for them, and re-layouts: 4.91 us -> 7.98 us
    all_to_all x4 -> x3, blocking collectives: 90.2 us -> 38.6 us  [exchange(): return lax.all_to_all(blocks, axis, split_axis=0, concat_axis=0, tiled=True)]
    all_gather x0 -> x3, waiting for transfers between devices: none -> 50.1 us  [gathered(): lax.all_gather(jnp.concatenate(weights, axis=1), 'z', axis=0, tiled=True)]
    psum x2 -> x0, blocking collectives: 49.5 us -> none  [the longest x1 26 us: token_mixer(): branch = lax.psum(projected, 'tp').astype(jnp.float32)]
    all_gather x1 -> x0, blocking collectives: 16.2 us -> none  [body(): columns = lax.all_gather(residual_in, 'tp', axis=1, tiled=True)]
    all_to_all x3 -> x5, starting transfers between devices: 21.5 us -> 33.7 us  [exchange(): return lax.all_to_all(blocks, axis, split_axis=0, concat_axis=0, tiled=True)]
    dot_general x7 -> x6, matrix products: 3.83 us -> 9.88 us  [the longest x3 4.25 us: times_transposed(): lax.dot_general(left, right_rows, (((1,), (1,)), ((), ())), preferred_ele...]
    all_to_all x3 -> x5, waiting for transfers between devices: 36.3 us -> 32.6 us  [exchange(): return lax.all_to_all(blocks, axis, split_axis=0, concat_axis=0, tiled=True)]
    concatenate x2 -> x7, other arithmetic: 0.12 us -> 3.3 us  [the longest x2 2.51 us: gathered(): jnp.concatenate(weights, axis=1)]
  transfers between devices with their start and end apart: 3 -> 8, of which waited for: 3 -> 8; matrix products, arithmetic and copies ran while one was open for 0% -> 9% of each run, Pallas kernels for 0% -> 0%
where the time goes in v1:
time: 201 us; the launch traced here: 200 us
  waiting for transfers between devices  82.7 us (41%)
  blocking collectives  38.6 us (19%)
  starting transfers between devices  33.8 us (17%)
  between operations  14.1 us (7%)
  matrix products  13.8 us (7%)
  other arithmetic  8.8 us (4%)
  local copies, waits for them, and re-layouts  7.98 us (4%)
    all_gather x3, waiting for transfers between devices, gathered(): lax.all_gather(jnp.concatenate(weights, axis=1), 'z', axis=0, tiled=True)  50.1 us
    all_to_all x3, blocking collectives, exchange(): return lax.all_to_all(blocks, axis, split_axis=0, concat_axis=0, tiled=True)  38.6 us
    all_to_all x5, starting transfers between devices, exchange(): return lax.all_to_all(blocks, axis, split_axis=0, concat_axis=0, tiled=True)  33.7 us
    all_to_all x5, waiting for transfers between devices, exchange(): return lax.all_to_all(blocks, axis, split_axis=0, concat_axis=0, tiled=True)  32.6 us
    dot_general x3, matrix products, times_transposed(): lax.dot_general(left, right_rows, (((1,), (1,)), ((), ())), preferred_ele...  4.25 us
  transfers between devices with their start and end apart: 8, of which 8 were waited for; matrix products, arithmetic and copies ran while one was open for 9% of the time, Pallas kernels for 0%

profile of v1, /device:TPU:1, one launch (start us, length us, event | category | flops | bytes accessed | tf_op | source)
XLA Modules:
  0.0 199.8 jit_solution(17900534135852283089)
XLA Ops:
  7.2 1.7 multiply_convert_fusion.1
  9.0 0.7 constant_dynamic-slice_fusion
  9.7 0.1 copy.77
  9.8 0.1 copy.78
  10.0 1.0 concatenate.43
  11.0 0.8 multiply_convert_fusion
  11.7 1.8 pad_maximum_fusion.1
  13.5 0.1 reshape.109
  13.7 0.7 reshape.127
  14.4 13.0 %all-to-all-start = ((bf16[64,2,128]{2,1,0:T(2,128)(2,1)}), bf16[64,2,128]{2,1,0:T(2,128)(2,1)S(1)}, u32[]{:S(2)}, u32[]{:S(2)}) async-start(bf16[64,2,128]{2,1,0:T(2,128)(2,1)} %reshape.127), calls=%async_computation | async-start | bytes 65536 | tf_op jit(solution)/shard_map/all_to_all | solution.py:21
  27.4 9.5 %all-to-all-done = bf16[64,2,128]{2,1,0:T(2,128)(2,1)S(1)} async-done(((bf16[64,2,128]{2,1,0:T(2,128)(2,1)}), bf16[64,2,128]{2,1,0:T(2,128)(2,1)S(1)}, u32[]{:S(2)}, u32[]{:S(2)}) %all-to-all-start) | async-done | bytes 32800 | tf_op jit(solution)/shard_map/all_to_all | solution.py:21
  36.9 0.1 reshape.128
  37.0 0.1 copy.76
  37.1 0.1 fusion.19
  37.2 0.1 select_convert_fusion.1
  37.3 12.2 %all-gather.6.cloned.1.call-done = bf16[512,1408]{1,0:T(8,128)(2,1)} async-done(((bf16[64,1408]{1,0:T(8,128)(2,1)}), bf16[512,1408]{1,0:T(8,128)(2,1)}) %all-gather.6.cloned.1.call-update) | async-done | bytes 1441808 | tf_op jit(solution)/shard_map/all_gather | solution.py:137
  49.6 1.7 fusion
  51.3 0.8 broadcast_in_dim.91
  52.1 4.2 %all-to-all-start.1 = ((bf16[4,32,1536]{2,1,0:T(8,128)(2,1)}), bf16[4,32,1536]{2,1,0:T(8,128)(2,1)S(1)}, u32[]{:S(2)}, u32[]{:S(2)}) async-start(bf16[4,32,1536]{2,1,0:T(8,128)(2,1)} %broadcast_in_dim.91), calls=%async_computation.1 | async-start | bytes 786432 | tf_op jit(solution)/shard_map/all_to_all | solution.py:21
  56.3 0.1 multiply_convert_fusion.2
  56.4 6.1 %all-to-all-done.1 = bf16[4,32,1536]{2,1,0:T(8,128)(2,1)S(1)} async-done(((bf16[4,32,1536]{2,1,0:T(8,128)(2,1)}), bf16[4,32,1536]{2,1,0:T(8,128)(2,1)S(1)}, u32[]{:S(2)}, u32[]{:S(2)}) %all-to-all-start.1) | async-done | bytes 393248 | tf_op jit(solution)/shard_map/all_to_all | solution.py:21
  62.6 0.2 fusion.41
  62.8 29.2 %all-gather.8.cloned.1.call-done = bf16[512,2368]{1,0:T(8,128)(2,1)} async-done(((bf16[64,2368]{1,0:T(8,128)(2,1)}), bf16[512,2368]{1,0:T(8,128)(2,1)}) %all-gather.8.cloned.1.call-update) | async-done | bytes 2424848 | tf_op jit(solution)/shard_map/all_gather | solution.py:137
  91.9 1.5 convolution_convert_fusion.3
  93.4 0.7 broadcast_in_dim.93
  94.2 8.7 %all-to-all-start.2 = ((bf16[8,32,512]{2,1,0:T(8,128)(2,1)}), bf16[8,32,512]{2,1,0:T(8,128)(2,1)S(1)}, u32[]{:S(2)}, u32[]{:S(2)}) async-start(bf16[8,32,512]{2,1,0:T(8,128)(2,1)} %broadcast_in_dim.93), calls=%async_computation.2 | async-start | bytes 524288 | tf_op jit(solution)/shard_map/all_to_all | solution.py:21
  102.9 0.8 pad_maximum_fusion
  103.7 5.7 %all-to-all-done.2 = bf16[8,32,512]{2,1,0:T(8,128)(2,1)S(1)} async-done(((bf16[8,32,512]{2,1,0:T(8,128)(2,1)}), bf16[8,32,512]{2,1,0:T(8,128)(2,1)S(1)}, u32[]{:S(2)}, u32[]{:S(2)}) %all-to-all-start.2) | async-done | bytes 262176 | tf_op jit(solution)/shard_map/all_to_all | solution.py:21
  109.4 0.1 fusion.17
  109.5 0.1 select_select_fusion
  109.6 2.2 %fusion.3 = f32[32,1664]{1,0:T(8,128)S(1)} fusion(bf16[32,512]{1,0:T(8,128)(2,1)S(1)} %get-tuple-element.5, bf16[512,2368]{1,0:T(8,128)(2,1)} %all-gather.8.cloned.1.call-done), kind=kOutput, calls=%fused_computation.6 | convolution fusion | flops 54525952 | bytes 1949696 | tf_op jit(solution)/shard_map/dot_general | solution.py:74
  111.8 0.1 fusion.46
  111.9 0.7 pad_maximum_fusion.2
  112.6 4.0 %all-to-all-start.3 = ((bf16[4,8,1664]{2,1,0:T(8,128)(2,1)}), bf16[4,8,1664]{2,1,0:T(8,128)(2,1)S(1)}, u32[]{:S(2)}, u32[]{:S(2)}) async-start(bf16[4,8,1664]{2,1,0:T(8,128)(2,1)} %pad_maximum_fusion.2), calls=%async_computation.3 | async-start | bytes 212992 | tf_op jit(solution)/shard_map/all_to_all | solution.py:21
  116.6 4.7 %all-to-all-done.3 = bf16[4,8,1664]{2,1,0:T(8,128)(2,1)S(1)} async-done(((bf16[4,8,1664]{2,1,0:T(8,128)(2,1)}), bf16[4,8,1664]{2,1,0:T(8,128)(2,1)S(1)}, u32[]{:S(2)}, u32[]{:S(2)}) %all-to-all-start.3) | async-done | bytes 106528 | tf_op jit(solution)/shard_map/all_to_all | solution.py:21
  121.4 0.2 fusion.56
  121.5 0.1 slice_multiply_fusion.4
  121.6 0.1 fusion.47
  121.9 0.1 add_divide_fusion
  122.0 0.1 copy.80
  122.1 2.0 %fusion.1 = f32[8,4,1,128]{3,2,1,0:T(1,128)S(1)} fusion(f32[8,4,128,1]{2,3,1,0:T(1,128)S(1)} %bitcast.109, f32[8,4,128,128]{3,2,1,0:T(8,128)S(1)} %copy-done, f32[8,4]{1,0:T(8,128)S(1)} %get-tuple-element.9), kind=kOutput, calls=%fused_computation.4 | convolution fusion | flops 6815744 | bytes 2130048 | tf_op jit(solution)/shard_map/rhab,rha->rhb/dot_general | solution.py:65
  124.2 0.8 multiply_add_fusion
  125.0 1.3 copy-done.1
  126.3 1.9 fusion.65
  128.2 0.1 fusion.43
  128.3 0.1 fusion.50
  128.4 6.7 %all_to_all.40 = bf16[4,8,512]{2,1,0:T(8,128)(2,1)S(1)} all-to-all(bf16[4,8,512]{2,1,0:T(8,128)(2,1)S(1)} %broadcast_in_dim.98), channel_id=1, replica_groups=mesh['z'=8,'y'=4,'x'=4,'c'=2] {'y'}, dimensions={0} | all-to-all | bytes 65536 | tf_op jit(solution)/shard_map/all_to_all | solution.py:21
  135.1 8.7 %all-gather.4.cloned.1.call-done = bf16[512,2624]{1,0:T(8,128)(2,1)} async-done(((bf16[64,2624]{1,0:T(8,128)(2,1)}), bf16[512,2624]{1,0:T(8,128)(2,1)}) %all-gather.4.cloned.1.call-update) | async-done | bytes 2686992 | tf_op jit(solution)/shard_map/all_gather | solution.py:137
  143.8 1.3 convolution_convert_fusion.4
  145.2 13.9 %all_to_all.41 = bf16[8,32,512]{2,1,0:T(8,128)(2,1)S(1)} all-to-all(bf16[8,32,512]{2,1,0:T(8,128)(2,1)S(1)} %broadcast_in_dim.99), channel_id=1, replica_groups=mesh['z'=8,'y'=4,'x'=4,'c'=2] {'x','c'}, dimensions={0} | all-to-all | bytes 524288 | tf_op jit(solution)/shard_map/all_to_all | solution.py:21
  159.1 0.1 multiply_reduce_fusion
  159.3 0.1 select_convert_fusion
  159.4 1.7 convolution_convert_fusion
  161.1 0.8 broadcast_in_dim.102
  161.9 3.8 %all-to-all-start.6 = ((bf16[4,32,1536]{2,1,0:T(8,128)(2,1)}), bf16[4,32,1536]{2,1,0:T(8,128)(2,1)S(1)}, u32[]{:S(2)}, u32[]{:S(2)}) async-start(bf16[4,32,1536]{2,1,0:T(8,128)(2,1)} %broadcast_in_dim.102), calls=%async_computation.6 | async-start | bytes 786432 | tf_op jit(solution)/shard_map/all_to_all | solution.py:21
  165.7 6.5 %all-to-all-done.6 = bf16[4,32,1536]{2,1,0:T(8,128)(2,1)S(1)} async-done(((bf16[4,32,1536]{2,1,0:T(8,128)(2,1)}), bf16[4,32,1536]{2,1,0:T(8,128)(2,1)S(1)}, u32[]{:S(2)}, u32[]{:S(2)}) %all-to-all-start.6) | async-done | bytes 393248 | tf_op jit(solution)/shard_map/all_to_all | solution.py:21
  172.3 0.2 fusion.36
  172.5 1.5 convolution_convert_fusion.2
  174.0 0.1 copy.83
  174.2 0.2 reshape.129
  174.3 18.0 %all_to_all.42 = bf16[64,2,256]{2,1,0:T(2,128)(2,1)S(1)} all-to-all(bf16[64,2,256]{2,1,0:T(2,128)(2,1)S(1)} %reshape.129), channel_id=1, replica_groups=mesh['z'=8,'y'=4,'x'=4,'c'=2] {'z','x','c'}, dimensions={0} | all-to-all | bytes 131072 | tf_op jit(solution)/shard_map/all_to_all | solution.py:21
  192.3 0.1 reshape.130
  192.5 0.1 fusion.32
  192.6 0.7 convert_element_type.209
  (64 shorter events, 1.0 us)
Async XLA Ops:
  7.2 6.4 %copy-start.6 = (bf16[256,8]{0,1:T(8,128)(2,1)S(1)}, bf16[256,8]{0,1:T(8,128)(2,1)}, u32[]{:S(2)}) copy-start(bf16[256,8]{0,1:T(8,128)(2,1)} %param.21) | copy-start | bytes 12292
  7.2 42.4 %all-gather.6.cloned.1.call-start = ((), (), s32[]{:S(2)}) async-start(), calls=%async_computation.9 | async-start | bytes 1622016 | tf_op jit(solution)/shard_map/all_gather | solution.py:137
  9.0 83.0 %all-gather.8.cloned.1.call-start = ((), (), s32[]{:S(2)}) async-start(), calls=%async_computation.10 | async-start | bytes 2801664 | tf_op jit(solution)/shard_map/all_gather | solution.py:137
  13.5 42.8 %copy-start.2 = (bf16[64,704]{1,0:T(8,128)(2,1)S(1)}, bf16[64,704]{1,0:T(8,128)(2,1)}, u32[]{:S(2)}) copy-start(bf16[64,704]{1,0:T(8,128)(2,1)} %param.40) | copy-start | bytes 270340
  13.5 42.8 %copy-start.3 = (bf16[64,704]{1,0:T(8,128)(2,1)S(1)}, bf16[64,704]{1,0:T(8,128)(2,1)}, u32[]{:S(2)}) copy-start(bf16[64,704]{1,0:T(8,128)(2,1)} %param.39) | copy-start | bytes 270340
  13.5 42.8 %copy-start.7 = (f32[64]{0:T(128)S(1)}, f32[64]{0:T(128)}, u32[]{:S(2)}) copy-start(f32[64]{0:T(128)} %param.38) | copy-start | bytes 772
  14.4 22.5 %all-to-all-start = ((bf16[64,2,128]{2,1,0:T(2,128)(2,1)}), bf16[64,2,128]{2,1,0:T(2,128)(2,1)S(1)}, u32[]{:S(2)}, u32[]{:S(2)}) async-start(bf16[64,2,128]{2,1,0:T(2,128)(2,1)} %reshape.127), calls=%async_computation | async-start | bytes 65536 | tf_op jit(solution)/shard_map/all_to_all | solution.py:21
  52.1 50.8 %copy-start.4 = (bf16[704,64]{0,1:T(8,128)(2,1)S(1)}, bf16[704,64]{0,1:T(8,128)(2,1)}, u32[]{:S(2)}) copy-start(bf16[704,64]{0,1:T(8,128)(2,1)} %param.41) | copy-start | bytes 270340
  52.1 50.8 %copy-start.5 = (bf16[512,64]{0,1:T(8,128)(2,1)S(1)}, bf16[512,64]{0,1:T(8,128)(2,1)}, u32[]{:S(2)}) copy-start(bf16[512,64]{0,1:T(8,128)(2,1)} %param.37) | copy-start | bytes 196612
  52.1 10.5 %all-to-all-start.1 = ((bf16[4,32,1536]{2,1,0:T(8,128)(2,1)}), bf16[4,32,1536]{2,1,0:T(8,128)(2,1)S(1)}, u32[]{:S(2)}, u32[]{:S(2)}) async-start(bf16[4,32,1536]{2,1,0:T(8,128)(2,1)} %broadcast_in_dim.91), calls=%async_computation.1 | async-start | bytes 786432 | tf_op jit(solution)/shard_map/all_to_all | solution.py:21
  94.2 15.2 %all-to-all-start.2 = ((bf16[8,32,512]{2,1,0:T(8,128)(2,1)}), bf16[8,32,512]{2,1,0:T(8,128)(2,1)S(1)}, u32[]{:S(2)}, u32[]{:S(2)}) async-start(bf16[8,32,512]{2,1,0:T(8,128)(2,1)} %broadcast_in_dim.93), calls=%async_computation.2 | async-start | bytes 524288 | tf_op jit(solution)/shard_map/all_to_all | solution.py:21
  102.9 13.7 %copy-start.10 = (f32[4]{0:T(128)S(1)}, f32[4]{0:T(128)}, u32[]{:S(2)}) copy-start(f32[4]{0:T(128)} %param.34) | copy-start | bytes 52
  102.9 41.0 %all-gather.4.cloned.1.call-start = ((), (), s32[]{:S(2)}) async-start(), calls=%async_computation.8 | async-start | bytes 3096576 | tf_op jit(solution)/shard_map/all_gather | solution.py:137
  103.6 18.3 %copy-start.9 = (f32[4]{0:T(128)S(1)}, f32[4]{0:T(128)}, u32[]{:S(2)}) copy-start(f32[4]{0:T(128)} %param.35) | copy-start | bytes 52
  103.6 18.5 %copy-start = (f32[8,4,128,128]{3,2,1,0:T(8,128)S(1)}, f32[8,4,128,128]{3,2,1,0:T(8,128)}, u32[]{:S(2)}) copy-start(f32[8,4,128,128]{3,2,1,0:T(8,128)} %param.22) | copy-start | bytes 6291460
  112.6 8.8 %all-to-all-start.3 = ((bf16[4,8,1664]{2,1,0:T(8,128)(2,1)}), bf16[4,8,1664]{2,1,0:T(8,128)(2,1)S(1)}, u32[]{:S(2)}, u32[]{:S(2)}) async-start(bf16[4,8,1664]{2,1,0:T(8,128)(2,1)} %pad_maximum_fusion.2), calls=%async_computation.3 | async-start | bytes 212992 | tf_op jit(solution)/shard_map/all_to_all | solution.py:21
  125.0 1.3 copy-start.1
  125.0 3.3 %copy-start.8 = (f32[128]{0:T(128)S(1)}, f32[128]{0:T(128)}, u32[]{:S(2)}) copy-start(f32[128]{0:T(128)} %param.36) | copy-start | bytes 1540
  161.9 10.4 %all-to-all-start.6 = ((bf16[4,32,1536]{2,1,0:T(8,128)(2,1)}), bf16[4,32,1536]{2,1,0:T(8,128)(2,1)S(1)}, u32[]{:S(2)}, u32[]{:S(2)}) async-start(bf16[4,32,1536]{2,1,0:T(8,128)(2,1)} %broadcast_in_dim.102), calls=%async_computation.6 | async-start | bytes 786432 | tf_op jit(solution)/shard_map/all_to_all | solution.py:21
Sparse Core Ops, SparseCore 0:
  10.3 39.1 all-gather.5
  51.3 40.5 all-gather.7
  105.4 38.3 all-gather.3

commit v2 on v1

--- a/solution.py
+++ b/solution.py
@@ -44,11 +44,26 @@
     return lax.rsqrt((first_two[:, :1] + first_two[:, 1:2]) / D + epsilon)
 
 
-def hidden_units(residual, gate_up):
-    partial_value = jnp.dot(residual, gate_up, preferred_element_type=f32)
+def around(block, axis):
+    size = lax.axis_size(axis)
+    ahead = [(i, (i + 1) % size) for i in range(size)]
+    behind = [(i, (i - 1) % size) for i in range(size)]
+    blocks = [block] + [None] * (size - 1)
+    forward = backward = block
+    for step in range(1, size // 2):
+        forward = blocks[size - step] = lax.ppermute(forward, axis, ahead)
+        backward = blocks[step] = lax.ppermute(backward, axis, behind)
+    half = block.shape[1] // 2
+    forward = lax.ppermute(forward[:, :half], axis, ahead)
+    backward = lax.ppermute(backward[:, half:], axis, behind)
+    blocks[size // 2] = jnp.concatenate([forward, backward], axis=1)
+    return blocks
+
+
+def hidden_units(residual, partial_value):
     both = jnp.concatenate([partial_value, square_columns(residual.astype(f32))], axis=1).astype(bf16)
     summed = everyone_sum(both, "y")
-    width = gate_up.shape[1]
+    width = partial_value.shape[1]
     scale = row_scale(summed[:, width:])
     gate_act = summed[:, : width // 2] * scale
     up_act = summed[:, width // 2 : width] * scale
@@ -148,7 +163,7 @@
     )
     second_in = scaled_rows(norm_gain_second, [gate_second, up_second])
     width, mixer_width = first_in.shape[1], mixer_in.shape[1]
-    first_in = gathered([first_in])
+    first_blocks = around(first_in, "z")
     middle = gathered([down_first.T, mixer_in])
     last = gathered([out_weight.T, second_in, down_second.T])
     down_first, mixer_in = middle[:, : width // 2], middle[:, width // 2 :]
@@ -163,9 +178,20 @@
     own_cols, rows = columns.shape[0], columns.shape[1] // planes
     pieces = jnp.moveaxis(columns.reshape(own_cols, planes, rows), 1, 0)
     pieces = jnp.broadcast_to(pieces[:, None], (planes, tp_count, own_cols, rows))
-    residual = exchange(pieces.reshape(-1, own_cols, rows), ACROSS).reshape(-1, rows).T
-
-    hidden = hidden_units(residual, first_in)
+    arrived = exchange(pieces.reshape(-1, own_cols, rows), ACROSS).reshape(planes, -1, rows)
+    residual = arrived.reshape(-1, rows).T
+    twice = jnp.concatenate([arrived, arrived], axis=0)
+    ahead = lax.dynamic_slice_in_dim(twice, lax.axis_index("z"), planes, 0)
+    products = [
+        lax.dot_general(ahead[o], first_blocks[o], (((0,), (0,)), ((), ())), preferred_element_type=f32)
+        for step in range(planes // 2 + 1)
+        for o in sorted({step, (planes - step) % planes})
+    ]
+    partial_value = products[0]
+    for product in products[1:]:
+        partial_value = partial_value + product
+
+    hidden = hidden_units(residual, partial_value)
     projected = times_transposed(hidden, down_first).astype(bf16)
     after_first = (residual.astype(f32) + 0.5 * everyone_sum(projected, TP)).astype(bf16)
 
@@ -176,7 +202,7 @@
     projected = times_transposed(normed, out_rows).astype(bf16)
     after_mixer = (after_first.astype(f32) + everyone_sum(projected, TP)).astype(bf16)
 
-    hidden = hidden_units(after_mixer, second_in)
+    hidden = hidden_units(after_mixer, jnp.dot(after_mixer, second_in, preferred_element_type=f32))
     projected = times_transposed(down_second, hidden).astype(bf16)
     pieces = jnp.concatenate([projected, after_mixer.T], axis=1)
     arrived = exchange(pieces.reshape(-1, own_cols, 2 * rows), ACROSS)

time: 201 us -> 184 us (0.915)
  waiting for transfers between devices: 82.7 us -> 57.8 us
  starting transfers between devices: 33.8 us -> 43 us
    all_gather x3 -> x2, waiting for transfers between devices: 50.1 us -> 8.3 us  [gathered(): lax.all_gather(jnp.concatenate(weights, axis=1), 'z', axis=0, tiled=True)]
    ppermute x0 -> x8, waiting for transfers between devices: none -> 16.9 us  [the longest x3 15.2 us: around(): forward = blocks[size - step] = lax.ppermute(forward, axis, ahead)]
    ppermute x0 -> x8, starting transfers between devices: none -> 14.7 us  [the longest x3 11.5 us: around(): backward = blocks[step] = lax.ppermute(backward, axis, behind)]
    all_to_all x5, starting transfers between devices: 33.7 us -> 28.2 us  [exchange(): return lax.all_to_all(blocks, axis, split_axis=0, concat_axis=0, tiled=True)]
  transfers between devices with their start and end apart: 8 -> 15, of which waited for: 8 -> 9; matrix products, arithmetic and copies ran while one was open for 9% -> 8% of each run, Pallas kernels for 0% -> 0%
where the time goes in v2:
time: 184 us
  waiting for transfers between devices  57.8 us (31%)
  starting transfers between devices  43 us (23%)
  blocking collectives  38.3 us (21%)
  between operations  14.5 us (8%)
  matrix products  13.6 us (7%)
  other arithmetic  8.22 us (4%)
  local copies, waits for them, and re-layouts  8.11 us (4%)
    all_to_all x3, blocking collectives, exchange(): return lax.all_to_all(blocks, axis, split_axis=0, concat_axis=0, tiled=True)  38.3 us
    all_to_all x5, waiting for transfers between devices, exchange(): return lax.all_to_all(blocks, axis, split_axis=0, concat_axis=0, tiled=True)  32.6 us
    all_to_all x5, starting transfers between devices, exchange(): return lax.all_to_all(blocks, axis, split_axis=0, concat_axis=0, tiled=True)  28.2 us
    ppermute x3, waiting for transfers between devices, around(): forward = blocks[size - step] = lax.ppermute(forward, axis, ahead)  15.2 us
    ppermute x3, starting transfers between devices, around(): backward = blocks[step] = lax.ppermute(backward, axis, behind)  11.5 us
    all_gather x2, waiting for transfers between devices, gathered(): lax.all_gather(jnp.concatenate(weights, axis=1), 'z', axis=0, tiled=True)  8.3 us
    dot_general x3, matrix products, times_transposed(): lax.dot_general(left, right_rows, (((1,), (1,)), ((), ())), preferred_ele...  4.26 us
  transfers between devices with their start and end apart: 15, of which 9 were waited for; matrix products, arithmetic and copies ran while one was open for 8% of the time, Pallas kernels for 0%

profile of v2, /device:TPU:1, one launch (start us, length us, event | category | flops | bytes accessed | tf_op | source)
XLA Modules:
  0.0 183.5 jit_solution(5318345786310595501)
XLA Ops:
  7.2 0.7 constant_dynamic-slice_fusion
  7.9 0.1 copy.121
  8.1 0.1 copy.122
  8.2 1.0 concatenate.51
  9.2 0.8 multiply_convert_fusion
  9.9 1.7 pad_maximum_fusion.1
  11.7 1.0 multiply_convert_fusion.1
  12.8 6.5 %collective-permute-start = (bf16[64,1408]{1,0:T(8,128)(2,1)S(1)}, bf16[64,1408]{1,0:T(8,128)(2,1)S(1)}, u32[]{:S(2)}, u32[]{:S(2)}) collective-permute-start(bf16[64,1408]{1,0:T(8,128)(2,1)S(1)} %multiply_convert_fusion.1), channel_id=1, source_target_pairs={{0,224},{32,0},{64,32},{96,64},{128,96},{160,128},{192,160},{224,1... | collective-permute-start | bytes 540680 | tf_op jit(solution)/shard_map/ppermute | solution.py:55
  19.4 0.7 reshape.133
  20.1 8.6 %all-to-all-start = ((bf16[64,2,128]{2,1,0:T(2,128)(2,1)}), bf16[64,2,128]{2,1,0:T(2,128)(2,1)S(1)}, u32[]{:S(2)}, u32[]{:S(2)}) async-start(bf16[64,2,128]{2,1,0:T(2,128)(2,1)} %reshape.133), calls=%async_computation | async-start | bytes 65536 | tf_op jit(solution)/shard_map/all_to_all | solution.py:21
  28.7 9.7 %all-to-all-done = bf16[64,2,128]{2,1,0:T(2,128)(2,1)S(1)} async-done(((bf16[64,2,128]{2,1,0:T(2,128)(2,1)}), bf16[64,2,128]{2,1,0:T(2,128)(2,1)S(1)}, u32[]{:S(2)}, u32[]{:S(2)}) %all-to-all-start) | async-done | bytes 32800 | tf_op jit(solution)/shard_map/all_to_all | solution.py:21
  38.5 0.1 reshape.134
  38.7 0.1 fusion.27
  38.9 0.2 fusion.50
  39.2 0.4 collective-permute-start.3
  39.6 2.4 %collective-permute-start.2 = (bf16[64,1408]{1,0:T(8,128)(2,1)S(1)}, bf16[64,1408]{1,0:T(8,128)(2,1)S(1)}, u32[]{:S(2)}, u32[]{:S(2)}) collective-permute-start(bf16[64,1408]{1,0:T(8,128)(2,1)S(1)} %collective-permute-done), channel_id=1, source_target_pairs={{0,224},{32,0},{64,32},{96,64},{128,96},{160,128},{192,160},{224,1... | collective-permute-start | bytes 540680 | tf_op jit(solution)/shard_map/ppermute | solution.py:55
  42.0 0.2 convolution_add_fusion.3
  42.2 0.2 convolution_add_fusion.2
  42.4 8.1 %collective-permute-done.3 = bf16[64,1408]{1,0:T(8,128)(2,1)S(1)} collective-permute-done((bf16[64,1408]{1,0:T(8,128)(2,1)S(1)}, bf16[64,1408]{1,0:T(8,128)(2,1)S(1)}, u32[]{:S(2)}, u32[]{:S(2)}) %collective-permute-start.3) | collective-permute-done | bytes 180256 | tf_op jit(solution)/shard_map/ppermute | solution.py:54
  50.5 2.7 %collective-permute-start.4 = (bf16[64,1408]{1,0:T(8,128)(2,1)S(1)}, bf16[64,1408]{1,0:T(8,128)(2,1)S(1)}, u32[]{:S(2)}, u32[]{:S(2)}) collective-permute-start(bf16[64,1408]{1,0:T(8,128)(2,1)S(1)} %collective-permute-done.2), channel_id=1, source_target_pairs={{0,224},{32,0},{64,32},{96,64},{128,96},{160,128},{192,160},{224,1... | collective-permute-start | bytes 540680 | tf_op jit(solution)/shard_map/ppermute | solution.py:55
  53.1 0.2 fusion.49
  53.4 0.2 fusion.2
  53.6 7.1 %collective-permute-done.5 = bf16[64,1408]{1,0:T(8,128)(2,1)S(1)} collective-permute-done((bf16[64,1408]{1,0:T(8,128)(2,1)S(1)}, bf16[64,1408]{1,0:T(8,128)(2,1)S(1)}, u32[]{:S(2)}, u32[]{:S(2)}) %collective-permute-start.5) | collective-permute-done | bytes 180256 | tf_op jit(solution)/shard_map/ppermute | solution.py:54
  60.9 2.7 %collective-permute-start.7 = (bf16[64,704]{1,0:T(8,128)(2,1)S(1)}, bf16[64,704]{1,0:T(8,128)(2,1)S(1)}, u32[]{:S(2)}, u32[]{:S(2)}) collective-permute-start(bf16[64,704]{1,0:T(8,128)(2,1)S(1)} %slice.179), channel_id=1, source_target_pairs={{0,224},{32,0},{64,32},{96,64},{128,96},{160,128},{192,160},{224,1... | collective-permute-start | bytes 270344 | tf_op jit(solution)/shard_map/ppermute | solution.py:58
  63.7 0.2 fusion.48
  63.9 1.6 collective-permute-done.6
  65.5 0.2 fusion.13
  65.7 0.2 fusion.3
  66.0 0.8 broadcast_in_dim.91
  66.7 4.2 %all-to-all-start.1 = ((bf16[4,32,1536]{2,1,0:T(8,128)(2,1)}), bf16[4,32,1536]{2,1,0:T(8,128)(2,1)S(1)}, u32[]{:S(2)}, u32[]{:S(2)}) async-start(bf16[4,32,1536]{2,1,0:T(8,128)(2,1)} %broadcast_in_dim.91), calls=%async_computation.1 | async-start | bytes 786432 | tf_op jit(solution)/shard_map/all_to_all | solution.py:21
  71.0 0.1 multiply_convert_fusion.2
  71.1 6.1 %all-to-all-done.1 = bf16[4,32,1536]{2,1,0:T(8,128)(2,1)S(1)} async-done(((bf16[4,32,1536]{2,1,0:T(8,128)(2,1)}), bf16[4,32,1536]{2,1,0:T(8,128)(2,1)S(1)}, u32[]{:S(2)}, u32[]{:S(2)}) %all-to-all-start.1) | async-done | bytes 393248 | tf_op jit(solution)/shard_map/all_to_all | solution.py:21
  77.3 0.2 fusion.47
  77.5 1.5 convolution_convert_fusion.2
  79.0 0.7 broadcast_in_dim.93
  79.7 7.7 %all-to-all-start.2 = ((bf16[8,32,512]{2,1,0:T(8,128)(2,1)}), bf16[8,32,512]{2,1,0:T(8,128)(2,1)S(1)}, u32[]{:S(2)}, u32[]{:S(2)}) async-start(bf16[8,32,512]{2,1,0:T(8,128)(2,1)} %broadcast_in_dim.93), calls=%async_computation.2 | async-start | bytes 524288 | tf_op jit(solution)/shard_map/all_to_all | solution.py:21
  87.5 0.8 pad_maximum_fusion
  88.2 5.7 %all-to-all-done.2 = bf16[8,32,512]{2,1,0:T(8,128)(2,1)S(1)} async-done(((bf16[8,32,512]{2,1,0:T(8,128)(2,1)}), bf16[8,32,512]{2,1,0:T(8,128)(2,1)S(1)}, u32[]{:S(2)}, u32[]{:S(2)}) %all-to-all-start.2) | async-done | bytes 262176 | tf_op jit(solution)/shard_map/all_to_all | solution.py:21
  94.0 0.1 fusion.23
  94.2 2.2 %fusion.6 = f32[32,1664]{1,0:T(8,128)S(1)} fusion(bf16[32,512]{1,0:T(8,128)(2,1)S(1)} %get-tuple-element.5, bf16[512,2368]{1,0:T(8,128)(2,1)} %all-gather.5.cloned.1.call-done), kind=kOutput, calls=%fused_computation.12 | convolution fusion | flops 54525952 | bytes 1949696 | tf_op jit(solution)/shard_map/dot_general | solution.py:89
  96.5 0.7 pad_maximum_fusion.2
  97.2 3.5 %all-to-all-start.3 = ((bf16[4,8,1664]{2,1,0:T(8,128)(2,1)}), bf16[4,8,1664]{2,1,0:T(8,128)(2,1)S(1)}, u32[]{:S(2)}, u32[]{:S(2)}) async-start(bf16[4,8,1664]{2,1,0:T(8,128)(2,1)} %pad_maximum_fusion.2), calls=%async_computation.3 | async-start | bytes 212992 | tf_op jit(solution)/shard_map/all_to_all | solution.py:21
  100.7 4.5 %all-to-all-done.3 = bf16[4,8,1664]{2,1,0:T(8,128)(2,1)S(1)} async-done(((bf16[4,8,1664]{2,1,0:T(8,128)(2,1)}), bf16[4,8,1664]{2,1,0:T(8,128)(2,1)S(1)}, u32[]{:S(2)}, u32[]{:S(2)}) %all-to-all-start.3) | async-done | bytes 106528 | tf_op jit(solution)/shard_map/all_to_all | solution.py:21
  105.2 0.2 fusion.65
  106.0 2.0 %fusion.4 = f32[8,4,1,128]{3,2,1,0:T(1,128)S(1)} fusion(f32[8,4,128,1]{2,3,1,0:T(1,128)S(1)} %bitcast.145, f32[8,4,128,128]{3,2,1,0:T(8,128)S(1)} %copy-done, f32[8,4]{1,0:T(8,128)S(1)} %get-tuple-element.9), kind=kOutput, calls=%fused_computation.10 | convolution fusion | flops 6815744 | bytes 2130048 | tf_op jit(solution)/shard_map/rhab,rha->rhb/dot_general | solution.py:80
  108.1 0.8 multiply_add_fusion
  108.9 1.3 copy-done.1
  110.2 1.9 %fusion.74 = f32[8,4,1,128]{3,2,1,0:T(1,128)S(1)} fusion(f32[8,4,128,128]{3,2,1,0:T(8,128)S(1)} %multiply_add_fusion, f32[8,4,128,1]{2,3,1,0:T(1,128)S(1)} %bitcast.150), kind=kOutput, calls=%fused_computation.151 | convolution fusion | flops 6291456 | bytes 2129920 | tf_op jit(solution)/shard_map/rhab,rha->rhb/dot_general | solution.py:83
  112.2 6.7 %all_to_all.40 = bf16[4,8,512]{2,1,0:T(8,128)(2,1)S(1)} all-to-all(bf16[4,8,512]{2,1,0:T(8,128)(2,1)S(1)} %broadcast_in_dim.98), channel_id=1, replica_groups=mesh['z'=8,'y'=4,'x'=4,'c'=2] {'y'}, dimensions={0} | all-to-all | bytes 65536 | tf_op jit(solution)/shard_map/all_to_all | solution.py:21
  119.0 8.3 %all-gather.3.cloned.1.call-done = bf16[512,2624]{1,0:T(8,128)(2,1)} async-done(((bf16[64,2624]{1,0:T(8,128)(2,1)}), bf16[512,2624]{1,0:T(8,128)(2,1)}) %all-gather.3.cloned.1.call-update) | async-done | bytes 2686992 | tf_op jit(solution)/shard_map/all_gather | solution.py:152
  127.2 1.3 convolution_convert_fusion.3
  128.6 13.7 %all_to_all.41 = bf16[8,32,512]{2,1,0:T(8,128)(2,1)S(1)} all-to-all(bf16[8,32,512]{2,1,0:T(8,128)(2,1)S(1)} %broadcast_in_dim.99), channel_id=1, replica_groups=mesh['z'=8,'y'=4,'x'=4,'c'=2] {'x','c'}, dimensions={0} | all-to-all | bytes 524288 | tf_op jit(solution)/shard_map/all_to_all | solution.py:21
  142.3 0.1 multiply_reduce_fusion
  142.5 1.7 convolution_convert_fusion
  144.2 0.8 broadcast_in_dim.102
  145.0 4.1 %all-to-all-start.6 = ((bf16[4,32,1536]{2,1,0:T(8,128)(2,1)}), bf16[4,32,1536]{2,1,0:T(8,128)(2,1)S(1)}, u32[]{:S(2)}, u32[]{:S(2)}) async-start(bf16[4,32,1536]{2,1,0:T(8,128)(2,1)} %broadcast_in_dim.102), calls=%async_computation.6 | async-start | bytes 786432 | tf_op jit(solution)/shard_map/all_to_all | solution.py:21
  149.2 6.5 %all-to-all-done.6 = bf16[4,32,1536]{2,1,0:T(8,128)(2,1)S(1)} async-done(((bf16[4,32,1536]{2,1,0:T(8,128)(2,1)}), bf16[4,32,1536]{2,1,0:T(8,128)(2,1)S(1)}, u32[]{:S(2)}, u32[]{:S(2)}) %all-to-all-start.6) | async-done | bytes 393248 | tf_op jit(solution)/shard_map/all_to_all | solution.py:21
  155.8 0.2 fusion.42
  156.0 1.5 convolution_convert_fusion.1
  157.5 0.1 copy.128
  157.6 0.2 reshape.135
  157.8 17.9 %all_to_all.42 = bf16[64,2,256]{2,1,0:T(2,128)(2,1)S(1)} all-to-all(bf16[64,2,256]{2,1,0:T(2,128)(2,1)S(1)} %reshape.135), channel_id=1, replica_groups=mesh['z'=8,'y'=4,'x'=4,'c'=2] {'z','x','c'}, dimensions={0} | all-to-all | bytes 131072 | tf_op jit(solution)/shard_map/all_to_all | solution.py:21
  175.7 0.1 reshape.136
  176.0 0.7 convert_element_type.214
  (88 shorter events, 2.4 us)
Async XLA Ops:
  7.2 12.1 %copy-start.6 = (bf16[256,8]{0,1:T(8,128)(2,1)S(1)}, bf16[256,8]{0,1:T(8,128)(2,1)}, u32[]{:S(2)}) copy-start(bf16[256,8]{0,1:T(8,128)(2,1)} %param.21) | copy-start | bytes 12292
  7.2 70.3 %all-gather.5.cloned.1.call-start = ((), (), s32[]{:S(2)}) async-start(), calls=%async_computation.9 | async-start | bytes 2801664 | tf_op jit(solution)/shard_map/all_gather | solution.py:152
  12.8 26.8 %collective-permute-start = (bf16[64,1408]{1,0:T(8,128)(2,1)S(1)}, bf16[64,1408]{1,0:T(8,128)(2,1)S(1)}, u32[]{:S(2)}, u32[]{:S(2)}) collective-permute-start(bf16[64,1408]{1,0:T(8,128)(2,1)S(1)} %multiply_convert_fusion.1), channel_id=1, source_target_pairs={{0,224},{32,0},{64,32},{96,64},{128,96},{160,128},{192,160},{224,1... | collective-permute-start | bytes 540680 | tf_op jit(solution)/shard_map/ppermute | solution.py:55
  19.2 20.0 %collective-permute-start.1 = (bf16[64,1408]{1,0:T(8,128)(2,1)S(1)}, bf16[64,1408]{1,0:T(8,128)(2,1)S(1)}, u32[]{:S(2)}, u32[]{:S(2)}) collective-permute-start(bf16[64,1408]{1,0:T(8,128)(2,1)S(1)} %multiply_convert_fusion.1), channel_id=1, source_target_pairs={{0,32},{32,64},{64,96},{96,128},{128,160},{160,192},{192,224},{224... | collective-permute-start | bytes 540680 | tf_op jit(solution)/shard_map/ppermute | solution.py:54
  20.1 18.4 %all-to-all-start = ((bf16[64,2,128]{2,1,0:T(2,128)(2,1)}), bf16[64,2,128]{2,1,0:T(2,128)(2,1)S(1)}, u32[]{:S(2)}, u32[]{:S(2)}) async-start(bf16[64,2,128]{2,1,0:T(2,128)(2,1)} %reshape.133), calls=%async_computation | async-start | bytes 65536 | tf_op jit(solution)/shard_map/all_to_all | solution.py:21
  39.2 11.2 %collective-permute-start.3 = (bf16[64,1408]{1,0:T(8,128)(2,1)S(1)}, bf16[64,1408]{1,0:T(8,128)(2,1)S(1)}, u32[]{:S(2)}, u32[]{:S(2)}) collective-permute-start(bf16[64,1408]{1,0:T(8,128)(2,1)S(1)} %collective-permute-done.1), channel_id=1, source_target_pairs={{0,32},{32,64},{64,96},{96,128},{128,160},{160,192},{192,224},{224... | collective-permute-start | bytes 540680 | tf_op jit(solution)/shard_map/ppermute | solution.py:54
  39.6 10.9 %collective-permute-start.2 = (bf16[64,1408]{1,0:T(8,128)(2,1)S(1)}, bf16[64,1408]{1,0:T(8,128)(2,1)S(1)}, u32[]{:S(2)}, u32[]{:S(2)}) collective-permute-start(bf16[64,1408]{1,0:T(8,128)(2,1)S(1)} %collective-permute-done), channel_id=1, source_target_pairs={{0,224},{32,0},{64,32},{96,64},{128,96},{160,128},{192,160},{224,1... | collective-permute-start | bytes 540680 | tf_op jit(solution)/shard_map/ppermute | solution.py:55
  50.5 10.3 %collective-permute-start.5 = (bf16[64,1408]{1,0:T(8,128)(2,1)S(1)}, bf16[64,1408]{1,0:T(8,128)(2,1)S(1)}, u32[]{:S(2)}, u32[]{:S(2)}) collective-permute-start(bf16[64,1408]{1,0:T(8,128)(2,1)S(1)} %collective-permute-done.3), channel_id=1, source_target_pairs={{0,32},{32,64},{64,96},{96,128},{128,160},{160,192},{192,224},{224... | collective-permute-start | bytes 540680 | tf_op jit(solution)/shard_map/ppermute | solution.py:54
  50.5 10.4 %collective-permute-start.4 = (bf16[64,1408]{1,0:T(8,128)(2,1)S(1)}, bf16[64,1408]{1,0:T(8,128)(2,1)S(1)}, u32[]{:S(2)}, u32[]{:S(2)}) collective-permute-start(bf16[64,1408]{1,0:T(8,128)(2,1)S(1)} %collective-permute-done.2), channel_id=1, source_target_pairs={{0,224},{32,0},{64,32},{96,64},{128,96},{160,128},{192,160},{224,1... | collective-permute-start | bytes 540680 | tf_op jit(solution)/shard_map/ppermute | solution.py:55
  53.3 17.6 %copy-start.2 = (bf16[64,704]{1,0:T(8,128)(2,1)S(1)}, bf16[64,704]{1,0:T(8,128)(2,1)}, u32[]{:S(2)}) copy-start(bf16[64,704]{1,0:T(8,128)(2,1)} %param.40) | copy-start | bytes 270340
  53.4 17.6 %copy-start.3 = (bf16[64,704]{1,0:T(8,128)(2,1)S(1)}, bf16[64,704]{1,0:T(8,128)(2,1)}, u32[]{:S(2)}) copy-start(bf16[64,704]{1,0:T(8,128)(2,1)} %param.39) | copy-start | bytes 270340
  53.4 17.6 %copy-start.7 = (f32[64]{0:T(128)S(1)}, f32[64]{0:T(128)}, u32[]{:S(2)}) copy-start(f32[64]{0:T(128)} %param.38) | copy-start | bytes 772
  60.7 4.8 %collective-permute-start.6 = (bf16[64,704]{1,0:T(8,128)(2,1)S(1)}, bf16[64,704]{1,0:T(8,128)(2,1)S(1)}, u32[]{:S(2)}, u32[]{:S(2)}) collective-permute-start(bf16[64,704]{1,0:T(8,128)(2,1)S(1)} %slice.178), channel_id=1, source_target_pairs={{0,32},{32,64},{64,96},{96,128},{128,160},{160,192},{192,224},{224... | collective-permute-start | bytes 270344 | tf_op jit(solution)/shard_map/ppermute | solution.py:57
  60.9 4.6 %collective-permute-start.7 = (bf16[64,704]{1,0:T(8,128)(2,1)S(1)}, bf16[64,704]{1,0:T(8,128)(2,1)S(1)}, u32[]{:S(2)}, u32[]{:S(2)}) collective-permute-start(bf16[64,704]{1,0:T(8,128)(2,1)S(1)} %slice.179), channel_id=1, source_target_pairs={{0,224},{32,0},{64,32},{96,64},{128,96},{160,128},{192,160},{224,1... | collective-permute-start | bytes 270344 | tf_op jit(solution)/shard_map/ppermute | solution.py:58
  66.7 20.7 %copy-start.4 = (bf16[704,64]{0,1:T(8,128)(2,1)S(1)}, bf16[704,64]{0,1:T(8,128)(2,1)}, u32[]{:S(2)}) copy-start(bf16[704,64]{0,1:T(8,128)(2,1)} %param.41) | copy-start | bytes 270340
  66.7 20.7 %copy-start.5 = (bf16[512,64]{0,1:T(8,128)(2,1)S(1)}, bf16[512,64]{0,1:T(8,128)(2,1)}, u32[]{:S(2)}) copy-start(bf16[512,64]{0,1:T(8,128)(2,1)} %param.37) | copy-start | bytes 196612
  66.7 10.5 %all-to-all-start.1 = ((bf16[4,32,1536]{2,1,0:T(8,128)(2,1)}), bf16[4,32,1536]{2,1,0:T(8,128)(2,1)S(1)}, u32[]{:S(2)}, u32[]{:S(2)}) async-start(bf16[4,32,1536]{2,1,0:T(8,128)(2,1)} %broadcast_in_dim.91), calls=%async_computation.1 | async-start | bytes 786432 | tf_op jit(solution)/shard_map/all_to_all | solution.py:21
  79.7 14.2 %all-to-all-start.2 = ((bf16[8,32,512]{2,1,0:T(8,128)(2,1)}), bf16[8,32,512]{2,1,0:T(8,128)(2,1)S(1)}, u32[]{:S(2)}, u32[]{:S(2)}) async-start(bf16[8,32,512]{2,1,0:T(8,128)(2,1)} %broadcast_in_dim.93), calls=%async_computation.2 | async-start | bytes 524288 | tf_op jit(solution)/shard_map/all_to_all | solution.py:21
  87.4 39.8 %all-gather.3.cloned.1.call-start = ((), (), s32[]{:S(2)}) async-start(), calls=%async_computation.8 | async-start | bytes 3096576 | tf_op jit(solution)/shard_map/all_gather | solution.py:152
  87.4 13.2 %copy-start.10 = (f32[4]{0:T(128)S(1)}, f32[4]{0:T(128)}, u32[]{:S(2)}) copy-start(f32[4]{0:T(128)} %param.34) | copy-start | bytes 52
  88.2 17.6 %copy-start.9 = (f32[4]{0:T(128)S(1)}, f32[4]{0:T(128)}, u32[]{:S(2)}) copy-start(f32[4]{0:T(128)} %param.35) | copy-start | bytes 52
  88.2 17.8 %copy-start = (f32[8,4,128,128]{3,2,1,0:T(8,128)S(1)}, f32[8,4,128,128]{3,2,1,0:T(8,128)}, u32[]{:S(2)}) copy-start(f32[8,4,128,128]{3,2,1,0:T(8,128)} %param.22) | copy-start | bytes 6291460
  97.2 8.0 %all-to-all-start.3 = ((bf16[4,8,1664]{2,1,0:T(8,128)(2,1)}), bf16[4,8,1664]{2,1,0:T(8,128)(2,1)S(1)}, u32[]{:S(2)}, u32[]{:S(2)}) async-start(bf16[4,8,1664]{2,1,0:T(8,128)(2,1)} %pad_maximum_fusion.2), calls=%async_computation.3 | async-start | bytes 212992 | tf_op jit(solution)/shard_map/all_to_all | solution.py:21
  108.9 1.3 copy-start.1
  108.9 3.3 %copy-start.8 = (f32[128]{0:T(128)S(1)}, f32[128]{0:T(128)}, u32[]{:S(2)}) copy-start(f32[128]{0:T(128)} %param.36) | copy-start | bytes 1540
  145.0 10.7 %all-to-all-start.6 = ((bf16[4,32,1536]{2,1,0:T(8,128)(2,1)}), bf16[4,32,1536]{2,1,0:T(8,128)(2,1)S(1)}, u32[]{:S(2)}, u32[]{:S(2)}) async-start(bf16[4,32,1536]{2,1,0:T(8,128)(2,1)} %broadcast_in_dim.102), calls=%async_computation.6 | async-start | bytes 786432 | tf_op jit(solution)/shard_map/all_to_all | solution.py:21
Sparse Core Ops, SparseCore 0:
  11.8 50.4 all-gather.4
  90.0 37.1 all-gather.2

commit v3 on v2

--- a/solution.py
+++ b/solution.py
@@ -27,6 +27,14 @@
 
 def everyone_sum(value, axis):
     return from_everyone(value, axis).astype(f32).sum(axis=0)
+
+
+def ring_sum(value, axis):
+    size = lax.axis_size(axis)
+    total = value.astype(f32)
+    for places in range(1, size):
+        total = total + lax.ppermute(value, axis, [(i, (i + places) % size) for i in range(size)]).astype(f32)
+    return total
 
 
 def times_transposed(left, right_rows):
@@ -62,7 +70,7 @@
 
 def hidden_units(residual, partial_value):
     both = jnp.concatenate([partial_value, square_columns(residual.astype(f32))], axis=1).astype(bf16)
-    summed = everyone_sum(both, "y")
+    summed = ring_sum(both, "y")
     width = partial_value.shape[1]
     scale = row_scale(summed[:, width:])
     gate_act = summed[:, : width // 2] * scale
@@ -158,15 +166,22 @@
         jnp.zeros((beta_weight.shape[0], GATES - 2 * heads_dev), bf16),
     ]
     first_in = scaled_rows(norm_gain_first, [gate_first, up_first])
+    first_in, query_weight, gate_cols[0], gate_cols[1], down_first = lax.optimization_barrier(
+        (first_in, query_weight, gate_cols[0], gate_cols[1], down_first)
+    )
     mixer_in = scaled_rows(
         norm_gain_mixer, [query_weight, key_weight, value_weight, output_gate_weight, *gate_cols]
     )
     second_in = scaled_rows(norm_gain_second, [gate_second, up_second])
     width, mixer_width = first_in.shape[1], mixer_in.shape[1]
     first_blocks = around(first_in, "z")
-    middle = gathered([down_first.T, mixer_in])
-    last = gathered([out_weight.T, second_in, down_second.T])
-    down_first, mixer_in = middle[:, : width // 2], middle[:, width // 2 :]
+    middle = jnp.concatenate([mixer_in, down_first.T], axis=1)
+    middle, residual_in = lax.optimization_barrier((middle, residual_in))
+    middle = gathered([middle])
+    mixer_in, down_first = middle[:, :mixer_width], middle[:, mixer_width:]
+    last = jnp.concatenate([out_weight.T, second_in, down_second.T], axis=1)
+    first_blocks[3], last = lax.optimization_barrier((first_blocks[3], last))
+    last = gathered([last])
     values_width = out_weight.shape[0]
     out_rows, second_in, down_second = (
         last[:, :values_width],
@@ -179,6 +194,9 @@
     pieces = jnp.moveaxis(columns.reshape(own_cols, planes, rows), 1, 0)
     pieces = jnp.broadcast_to(pieces[:, None], (planes, tp_count, own_cols, rows))
     arrived = exchange(pieces.reshape(-1, own_cols, rows), ACROSS).reshape(planes, -1, rows)
+    arrived, first_blocks[2], first_blocks[-2] = lax.optimization_barrier(
+        (arrived, first_blocks[2], first_blocks[-2])
+    )
     residual = arrived.reshape(-1, rows).T
     twice = jnp.concatenate([arrived, arrived], axis=0)
     ahead = lax.dynamic_slice_in_dim(twice, lax.axis_index("z"), planes, 0)

time: 184 us -> 179 us (0.973)
  waiting for transfers between devices: 57.8 us -> 50.2 us
  starting transfers between devices: 43 us -> 46.7 us
    all_to_all x5 -> x3, waiting for transfers between devices: 32.6 us -> 15.3 us  [exchange(): return lax.all_to_all(blocks, axis, split_axis=0, concat_axis=0, tiled=True)]
    ppermute x3, waiting for transfers between devices: 15.2 us -> 2.68 us  [around(): forward = blocks[size - step] = lax.ppermute(forward, axis, ahead)]
    all_gather x2, waiting for transfers between devices: 8.3 us -> 19.2 us  [gathered(): lax.all_gather(jnp.concatenate(weights, axis=1), 'z', axis=0, tiled=True)]
    ppermute x0 -> x6, starting transfers between devices: none -> 9.76 us  [ring_sum(): lax.ppermute(value, axis, [(i, (i + places) % size) for i in range(size)])]
    ppermute x0 -> x6, waiting for transfers between devices: none -> 8.19 us  [ring_sum(): lax.ppermute(value, axis, [(i, (i + places) % size) for i in range(size)])]
    all_to_all x5 -> x3, starting transfers between devices: 28.2 us -> 21 us  [exchange(): return lax.all_to_all(blocks, axis, split_axis=0, concat_axis=0, tiled=True)]
  transfers between devices with their start and end apart: 15 -> 19, of which waited for: 9 -> 13; matrix products, arithmetic and copies ran while one was open for 8% -> 10% of each run, Pallas kernels for 0% -> 0%
where the time goes in v3:
time: 179 us; the launch traced here: 178 us
  waiting for transfers between devices  50.2 us (28%)
  starting transfers between devices  46.7 us (26%)
  blocking collectives  37.6 us (21%)
  between operations  14.5 us (8%)
  matrix products  13.3 us (7%)
  other arithmetic  8.11 us (5%)
  local copies, waits for them, and re-layouts  7.3 us (4%)
    all_to_all x3, blocking collectives, exchange(): return lax.all_to_all(blocks, axis, split_axis=0, concat_axis=0, tiled=True)  37.6 us
    all_to_all x3, starting transfers between devices, exchange(): return lax.all_to_all(blocks, axis, split_axis=0, concat_axis=0, tiled=True)  21 us
    all_gather x2, waiting for transfers between devices, gathered(): lax.all_gather(jnp.concatenate(weights, axis=1), 'z', axis=0, tiled=True)  19.2 us
    all_to_all x3, waiting for transfers between devices, exchange(): return lax.all_to_all(blocks, axis, split_axis=0, concat_axis=0, tiled=True)  15.3 us
    ppermute x3, starting transfers between devices, around(): backward = blocks[step] = lax.ppermute(backward, axis, behind)  12 us
    ppermute x6, starting transfers between devices, ring_sum(): lax.ppermute(value, axis, [(i, (i + places) % size) for i in range(size)])  9.76 us
    ppermute x6, waiting for transfers between devices, ring_sum(): lax.ppermute(value, axis, [(i, (i + places) % size) for i in range(size)])  8.19 us
    dot_general x3, matrix products, times_transposed(): lax.dot_general(left, right_rows, (((1,), (1,)), ((), ())), preferred_ele...  4.26 us
  transfers between devices with their start and end apart: 19, of which 13 were waited for; matrix products, arithmetic and copies ran while one was open for 10% of the time, Pallas kernels for 0%

profile of v3, /device:TPU:1, one launch (start us, length us, event | category | flops | bytes accessed | tf_op | source)
XLA Modules:
  0.0 177.8 jit_solution(6247522800233867787)
XLA Ops:
  7.2 0.8 constant_dynamic-slice_fusion
  8.0 1.0 multiply_convert_fusion.2
  9.1 6.5 %collective-permute-start = (bf16[64,1408]{1,0:T(8,128)(2,1)S(1)}, bf16[64,1408]{1,0:T(8,128)(2,1)S(1)}, u32[]{:S(2)}, u32[]{:S(2)}) collective-permute-start(bf16[64,1408]{1,0:T(8,128)(2,1)S(1)} %multiply_convert_fusion.2), channel_id=1, source_target_pairs={{0,224},{32,0},{64,32},{96,64},{128,96},{160,128},{192,160},{224,1... | collective-permute-start | bytes 540680 | tf_op jit(solution)/shard_map/ppermute | solution.py:63
  15.8 1.0 concatenate.48
  16.8 0.8 multiply_convert_fusion
  17.5 1.6 pad_maximum_fusion.1
  19.2 0.8 reshape.114
  20.0 0.7 reshape.134
  20.7 8.6 %all-to-all-start = ((bf16[64,2,128]{2,1,0:T(2,128)(2,1)}), bf16[64,2,128]{2,1,0:T(2,128)(2,1)S(1)}, u32[]{:S(2)}, u32[]{:S(2)}) async-start(bf16[64,2,128]{2,1,0:T(2,128)(2,1)} %reshape.134), calls=%async_computation | async-start | bytes 65536 | tf_op jit(solution)/shard_map/all_to_all | solution.py:21
  29.4 0.7 all-gather.5.cloned.1.call-update
  30.2 2.9 %collective-permute-start.1 = (bf16[64,1408]{1,0:T(8,128)(2,1)S(1)}, bf16[64,1408]{1,0:T(8,128)(2,1)S(1)}, u32[]{:S(2)}, u32[]{:S(2)}) collective-permute-start(bf16[64,1408]{1,0:T(8,128)(2,1)S(1)} %collective-permute-done), channel_id=1, source_target_pairs={{0,224},{32,0},{64,32},{96,64},{128,96},{160,128},{192,160},{224,1... | collective-permute-start | bytes 540680 | tf_op jit(solution)/shard_map/ppermute | solution.py:63
  33.2 0.8 pad_maximum_fusion
  33.9 4.8 %all-to-all-done = bf16[64,2,128]{2,1,0:T(2,128)(2,1)S(1)} async-done(((bf16[64,2,128]{2,1,0:T(2,128)(2,1)}), bf16[64,2,128]{2,1,0:T(2,128)(2,1)S(1)}, u32[]{:S(2)}, u32[]{:S(2)}) %all-to-all-start) | async-done | bytes 32800 | tf_op jit(solution)/shard_map/all_to_all | solution.py:21
  38.9 0.9 collective-permute-done.4
  40.2 2.7 %collective-permute-start.2 = (bf16[64,1408]{1,0:T(8,128)(2,1)S(1)}, bf16[64,1408]{1,0:T(8,128)(2,1)S(1)}, u32[]{:S(2)}, u32[]{:S(2)}) collective-permute-start(bf16[64,1408]{1,0:T(8,128)(2,1)S(1)} %collective-permute-done.1), channel_id=1, source_target_pairs={{0,224},{32,0},{64,32},{96,64},{128,96},{160,128},{192,160},{224,1... | collective-permute-start | bytes 540680 | tf_op jit(solution)/shard_map/ppermute | solution.py:63
  42.9 0.2 fusion.50
  43.1 0.2 fusion.49
  43.3 0.2 convolution_add_fusion.3
  43.5 0.2 convolution_add_fusion.2
  43.7 0.2 fusion.2
  44.0 1.8 collective-permute-done.5
  46.0 3.8 %collective-permute-start.7 = (bf16[64,704]{1,0:T(8,128)(2,1)S(1)}, bf16[64,704]{1,0:T(8,128)(2,1)S(1)}, u32[]{:S(2)}, u32[]{:S(2)}) collective-permute-start(bf16[64,704]{1,0:T(8,128)(2,1)S(1)} %slice.179), channel_id=1, source_target_pairs={{0,224},{32,0},{64,32},{96,64},{128,96},{160,128},{192,160},{224,1... | collective-permute-start | bytes 270344 | tf_op jit(solution)/shard_map/ppermute | solution.py:66
  49.7 0.2 fusion.48
  49.9 3.0 %collective-permute-done.6 = bf16[64,704]{1,0:T(8,128)(2,1)S(1)} collective-permute-done((bf16[64,704]{1,0:T(8,128)(2,1)S(1)}, bf16[64,704]{1,0:T(8,128)(2,1)S(1)}, u32[]{:S(2)}, u32[]{:S(2)}) %collective-permute-start.6) | collective-permute-done | bytes 90144 | tf_op jit(solution)/shard_map/ppermute | solution.py:65
  52.9 0.5 collective-permute-done.7
  53.4 0.2 fusion.13
  53.6 0.2 fusion.3
  53.8 3.4 %collective-permute-start.10 = (bf16[32,1536]{1,0:T(8,128)(2,1)S(1)}, bf16[32,1536]{1,0:T(8,128)(2,1)S(1)}, u32[]{:S(2)}, u32[]{:S(2)}) collective-permute-start(bf16[32,1536]{1,0:T(8,128)(2,1)S(1)} %pad_maximum_fusion.3), channel_id=1, source_target_pairs={{0,24},{8,0},{16,8},{24,16},{1,25},{9,1},{17,9},{25,17},{2,26},{10... | collective-permute-start | bytes 294920 | tf_op jit(solution)/shard_map/ppermute | solution.py:36
  57.2 1.5 collective-permute-start.9
  58.7 0.2 collective-permute-done.10
  58.9 4.5 %collective-permute-done.8 = bf16[32,1536]{1,0:T(8,128)(2,1)S(1)} collective-permute-done((bf16[32,1536]{1,0:T(8,128)(2,1)S(1)}, bf16[32,1536]{1,0:T(8,128)(2,1)S(1)}, u32[]{:S(2)}, u32[]{:S(2)}) %collective-permute-start.8) | collective-permute-done | bytes 98336 | tf_op jit(solution)/shard_map/ppermute | solution.py:36
  63.4 0.2 fusion.47
  63.6 10.3 %all-gather.5.cloned.1.call-done = bf16[512,2368]{1,0:T(8,128)(2,1)} async-done(((bf16[64,2368]{1,0:T(8,128)(2,1)}), bf16[512,2368]{1,0:T(8,128)(2,1)}) %all-gather.5.cloned.1.call-update) | async-done | bytes 2424848 | tf_op jit(solution)/shard_map/all_gather | solution.py:160
  73.9 1.5 convolution_convert_fusion.2
  75.4 0.7 broadcast_in_dim.86
  76.1 8.1 %all-to-all-start.1 = ((bf16[8,32,512]{2,1,0:T(8,128)(2,1)}), bf16[8,32,512]{2,1,0:T(8,128)(2,1)S(1)}, u32[]{:S(2)}, u32[]{:S(2)}) async-start(bf16[8,32,512]{2,1,0:T(8,128)(2,1)} %broadcast_in_dim.86), calls=%async_computation.1 | async-start | bytes 524288 | tf_op jit(solution)/shard_map/all_to_all | solution.py:21
  84.3 0.7 all-gather.3.cloned.1.call-update
  85.0 5.7 %all-to-all-done.1 = bf16[8,32,512]{2,1,0:T(8,128)(2,1)S(1)} async-done(((bf16[8,32,512]{2,1,0:T(8,128)(2,1)}), bf16[8,32,512]{2,1,0:T(8,128)(2,1)S(1)}, u32[]{:S(2)}, u32[]{:S(2)}) %all-to-all-start.1) | async-done | bytes 262176 | tf_op jit(solution)/shard_map/all_to_all | solution.py:21
  90.8 0.1 fusion.23
  91.1 1.9 %fusion.6 = f32[32,1664]{1,0:T(8,128)S(1)} fusion(bf16[32,512]{1,0:T(8,128)(2,1)S(1)} %get-tuple-element.29, bf16[512,2368]{1,0:T(8,128)(2,1)} %all-gather.5.cloned.1.call-done), kind=kOutput, calls=%fused_computation.12 | convolution fusion | flops 54525952 | bytes 1949696 | tf_op jit(solution)/shard_map/dot_general | solution.py:97
  93.0 0.7 pad_maximum_fusion.2
  93.7 4.2 %all-to-all-start.2 = ((bf16[4,8,1664]{2,1,0:T(8,128)(2,1)}), bf16[4,8,1664]{2,1,0:T(8,128)(2,1)S(1)}, u32[]{:S(2)}, u32[]{:S(2)}) async-start(bf16[4,8,1664]{2,1,0:T(8,128)(2,1)} %pad_maximum_fusion.2), calls=%async_computation.2 | async-start | bytes 212992 | tf_op jit(solution)/shard_map/all_to_all | solution.py:21
  97.9 4.7 %all-to-all-done.2 = bf16[4,8,1664]{2,1,0:T(8,128)(2,1)S(1)} async-done(((bf16[4,8,1664]{2,1,0:T(8,128)(2,1)}), bf16[4,8,1664]{2,1,0:T(8,128)(2,1)S(1)}, u32[]{:S(2)}, u32[]{:S(2)}) %all-to-all-start.2) | async-done | bytes 106528 | tf_op jit(solution)/shard_map/all_to_all | solution.py:21
  102.7 0.2 fusion.65
  103.4 2.0 %fusion.4 = f32[8,4,1,128]{3,2,1,0:T(1,128)S(1)} fusion(f32[8,4,128,1]{2,3,1,0:T(1,128)S(1)} %bitcast.145, f32[8,4,128,128]{3,2,1,0:T(8,128)S(1)} %copy-done, f32[8,4]{1,0:T(8,128)S(1)} %get-tuple-element.35), kind=kOutput, calls=%fused_computation.10 | convolution fusion | flops 6815744 | bytes 2130048 | tf_op jit(solution)/shard_map/rhab,rha->rhb/dot_general | solution.py:88
  105.6 0.8 multiply_add_fusion
  106.4 1.3 copy-done.1
  107.6 1.9 %fusion.74 = f32[8,4,1,128]{3,2,1,0:T(1,128)S(1)} fusion(f32[8,4,128,128]{3,2,1,0:T(8,128)S(1)} %multiply_add_fusion, f32[8,4,128,1]{2,3,1,0:T(1,128)S(1)} %bitcast.150), kind=kOutput, calls=%fused_computation.151 | convolution fusion | flops 6291456 | bytes 2129920 | tf_op jit(solution)/shard_map/rhab,rha->rhb/dot_general | solution.py:91
  109.7 6.7 %all_to_all.30 = bf16[4,8,512]{2,1,0:T(8,128)(2,1)S(1)} all-to-all(bf16[4,8,512]{2,1,0:T(8,128)(2,1)S(1)} %broadcast_in_dim.91), channel_id=1, replica_groups=mesh['z'=8,'y'=4,'x'=4,'c'=2] {'y'}, dimensions={0} | all-to-all | bytes 65536 | tf_op jit(solution)/shard_map/all_to_all | solution.py:21
  116.4 8.9 %all-gather.3.cloned.1.call-done = bf16[512,2624]{1,0:T(8,128)(2,1)} async-done(((bf16[64,2624]{1,0:T(8,128)(2,1)}), bf16[512,2624]{1,0:T(8,128)(2,1)}) %all-gather.3.cloned.1.call-update) | async-done | bytes 2686992 | tf_op jit(solution)/shard_map/all_gather | solution.py:160
  125.3 1.3 convolution_convert_fusion.3
  126.6 13.8 %all_to_all.31 = bf16[8,32,512]{2,1,0:T(8,128)(2,1)S(1)} all-to-all(bf16[8,32,512]{2,1,0:T(8,128)(2,1)S(1)} %broadcast_in_dim.92), channel_id=1, replica_groups=mesh['z'=8,'y'=4,'x'=4,'c'=2] {'x','c'}, dimensions={0} | all-to-all | bytes 524288 | tf_op jit(solution)/shard_map/all_to_all | solution.py:21
  140.6 1.7 convolution_convert_fusion
  142.4 1.3 collective-permute-start.11
  143.7 2.6 %collective-permute-start.12 = (bf16[32,1536]{1,0:T(8,128)(2,1)S(1)}, bf16[32,1536]{1,0:T(8,128)(2,1)S(1)}, u32[]{:S(2)}, u32[]{:S(2)}) collective-permute-start(bf16[32,1536]{1,0:T(8,128)(2,1)S(1)} %pad_maximum_fusion.4), channel_id=1, source_target_pairs={{0,16},{8,24},{16,0},{24,8},{1,17},{9,25},{17,1},{25,9},{2,18},{10... | collective-permute-start | bytes 294920 | tf_op jit(solution)/shard_map/ppermute | solution.py:36
  146.3 1.0 collective-permute-start.13
  147.3 2.7 %collective-permute-done.12 = bf16[32,1536]{1,0:T(8,128)(2,1)S(1)} collective-permute-done((bf16[32,1536]{1,0:T(8,128)(2,1)S(1)}, bf16[32,1536]{1,0:T(8,128)(2,1)S(1)}, u32[]{:S(2)}, u32[]{:S(2)}) %collective-permute-start.12) | collective-permute-done | bytes 98336 | tf_op jit(solution)/shard_map/ppermute | solution.py:36
  150.0 0.9 collective-permute-done.13
  150.9 0.2 fusion.42
  151.1 1.5 convolution_convert_fusion.1
  152.7 0.2 reshape.136
  152.9 17.1 %all_to_all.32 = bf16[64,2,256]{2,1,0:T(2,128)(2,1)S(1)} all-to-all(bf16[64,2,256]{2,1,0:T(2,128)(2,1)S(1)} %reshape.136), channel_id=1, replica_groups=mesh['z'=8,'y'=4,'x'=4,'c'=2] {'z','x','c'}, dimensions={0} | all-to-all | bytes 131072 | tf_op jit(solution)/shard_map/all_to_all | solution.py:21
  170.0 0.1 reshape.137
  170.3 0.7 convert_element_type.238
  (91 shorter events, 3.1 us)
Async XLA Ops:
  7.2 22.9 %copy-start.6 = (f32[64]{0:T(128)S(1)}, f32[64]{0:T(128)}, u32[]{:S(2)}) copy-start(f32[64]{0:T(128)} %param.38) | copy-start | bytes 772
  7.2 22.9 %copy-start.3 = (bf16[64,704]{1,0:T(8,128)(2,1)S(1)}, bf16[64,704]{1,0:T(8,128)(2,1)}, u32[]{:S(2)}) copy-start(bf16[64,704]{1,0:T(8,128)(2,1)} %param.39) | copy-start | bytes 270340
  7.2 22.9 %copy-start.2 = (bf16[64,704]{1,0:T(8,128)(2,1)S(1)}, bf16[64,704]{1,0:T(8,128)(2,1)}, u32[]{:S(2)}) copy-start(bf16[64,704]{1,0:T(8,128)(2,1)} %param.40) | copy-start | bytes 270340
  7.2 25.9 %copy-start.5 = (bf16[512,64]{0,1:T(8,128)(2,1)S(1)}, bf16[512,64]{0,1:T(8,128)(2,1)}, u32[]{:S(2)}) copy-start(bf16[512,64]{0,1:T(8,128)(2,1)} %param.37) | copy-start | bytes 196612
  7.2 25.9 %copy-start.4 = (bf16[704,64]{0,1:T(8,128)(2,1)S(1)}, bf16[704,64]{0,1:T(8,128)(2,1)}, u32[]{:S(2)}) copy-start(bf16[704,64]{0,1:T(8,128)(2,1)} %param.41) | copy-start | bytes 270340
  9.1 21.2 %collective-permute-start = (bf16[64,1408]{1,0:T(8,128)(2,1)S(1)}, bf16[64,1408]{1,0:T(8,128)(2,1)S(1)}, u32[]{:S(2)}, u32[]{:S(2)}) collective-permute-start(bf16[64,1408]{1,0:T(8,128)(2,1)S(1)} %multiply_convert_fusion.2), channel_id=1, source_target_pairs={{0,224},{32,0},{64,32},{96,64},{128,96},{160,128},{192,160},{224,1... | collective-permute-start | bytes 540680 | tf_op jit(solution)/shard_map/ppermute | solution.py:63
  15.5 17.6 %collective-permute-start.3 = (bf16[64,1408]{1,0:T(8,128)(2,1)S(1)}, bf16[64,1408]{1,0:T(8,128)(2,1)S(1)}, u32[]{:S(2)}, u32[]{:S(2)}) collective-permute-start(bf16[64,1408]{1,0:T(8,128)(2,1)S(1)} %multiply_convert_fusion.2), channel_id=1, source_target_pairs={{0,32},{32,64},{64,96},{96,128},{128,160},{160,192},{192,224},{224... | collective-permute-start | bytes 540680 | tf_op jit(solution)/shard_map/ppermute | solution.py:62
  20.7 18.0 %all-to-all-start = ((bf16[64,2,128]{2,1,0:T(2,128)(2,1)}), bf16[64,2,128]{2,1,0:T(2,128)(2,1)S(1)}, u32[]{:S(2)}, u32[]{:S(2)}) async-start(bf16[64,2,128]{2,1,0:T(2,128)(2,1)} %reshape.134), calls=%async_computation | async-start | bytes 65536 | tf_op jit(solution)/shard_map/all_to_all | solution.py:21
  29.3 44.6 %all-gather.5.cloned.1.call-start = ((), (), s32[]{:S(2)}) async-start(), calls=%async_computation.7 | async-start | bytes 2801664 | tf_op jit(solution)/shard_map/all_gather | solution.py:160
  30.2 8.6 %collective-permute-start.1 = (bf16[64,1408]{1,0:T(8,128)(2,1)S(1)}, bf16[64,1408]{1,0:T(8,128)(2,1)S(1)}, u32[]{:S(2)}, u32[]{:S(2)}) collective-permute-start(bf16[64,1408]{1,0:T(8,128)(2,1)S(1)} %collective-permute-done), channel_id=1, source_target_pairs={{0,224},{32,0},{64,32},{96,64},{128,96},{160,128},{192,160},{224,1... | collective-permute-start | bytes 540680 | tf_op jit(solution)/shard_map/ppermute | solution.py:63
  33.1 6.7 %collective-permute-start.4 = (bf16[64,1408]{1,0:T(8,128)(2,1)S(1)}, bf16[64,1408]{1,0:T(8,128)(2,1)S(1)}, u32[]{:S(2)}, u32[]{:S(2)}) collective-permute-start(bf16[64,1408]{1,0:T(8,128)(2,1)S(1)} %collective-permute-done.3), channel_id=1, source_target_pairs={{0,32},{32,64},{64,96},{96,128},{128,160},{160,192},{192,224},{224... | collective-permute-start | bytes 540680 | tf_op jit(solution)/shard_map/ppermute | solution.py:62
  40.1 5.6 %collective-permute-start.5 = (bf16[64,1408]{1,0:T(8,128)(2,1)S(1)}, bf16[64,1408]{1,0:T(8,128)(2,1)S(1)}, u32[]{:S(2)}, u32[]{:S(2)}) collective-permute-start(bf16[64,1408]{1,0:T(8,128)(2,1)S(1)} %collective-permute-done.4), channel_id=1, source_target_pairs={{0,32},{32,64},{64,96},{96,128},{128,160},{160,192},{192,224},{224... | collective-permute-start | bytes 540680 | tf_op jit(solution)/shard_map/ppermute | solution.py:62
  40.2 5.6 %collective-permute-start.2 = (bf16[64,1408]{1,0:T(8,128)(2,1)S(1)}, bf16[64,1408]{1,0:T(8,128)(2,1)S(1)}, u32[]{:S(2)}, u32[]{:S(2)}) collective-permute-start(bf16[64,1408]{1,0:T(8,128)(2,1)S(1)} %collective-permute-done.1), channel_id=1, source_target_pairs={{0,224},{32,0},{64,32},{96,64},{128,96},{160,128},{192,160},{224,1... | collective-permute-start | bytes 540680 | tf_op jit(solution)/shard_map/ppermute | solution.py:63
  45.8 7.1 %collective-permute-start.6 = (bf16[64,704]{1,0:T(8,128)(2,1)S(1)}, bf16[64,704]{1,0:T(8,128)(2,1)S(1)}, u32[]{:S(2)}, u32[]{:S(2)}) collective-permute-start(bf16[64,704]{1,0:T(8,128)(2,1)S(1)} %slice.178), channel_id=1, source_target_pairs={{0,32},{32,64},{64,96},{96,128},{128,160},{160,192},{192,224},{224... | collective-permute-start | bytes 270344 | tf_op jit(solution)/shard_map/ppermute | solution.py:65
  46.0 7.4 %collective-permute-start.7 = (bf16[64,704]{1,0:T(8,128)(2,1)S(1)}, bf16[64,704]{1,0:T(8,128)(2,1)S(1)}, u32[]{:S(2)}, u32[]{:S(2)}) collective-permute-start(bf16[64,704]{1,0:T(8,128)(2,1)S(1)} %slice.179), channel_id=1, source_target_pairs={{0,224},{32,0},{64,32},{96,64},{128,96},{160,128},{192,160},{224,1... | collective-permute-start | bytes 270344 | tf_op jit(solution)/shard_map/ppermute | solution.py:66
  53.8 5.0 %collective-permute-start.10 = (bf16[32,1536]{1,0:T(8,128)(2,1)S(1)}, bf16[32,1536]{1,0:T(8,128)(2,1)S(1)}, u32[]{:S(2)}, u32[]{:S(2)}) collective-permute-start(bf16[32,1536]{1,0:T(8,128)(2,1)S(1)} %pad_maximum_fusion.3), channel_id=1, source_target_pairs={{0,24},{8,0},{16,8},{24,16},{1,25},{9,1},{17,9},{25,17},{2,26},{10... | collective-permute-start | bytes 294920 | tf_op jit(solution)/shard_map/ppermute | solution.py:36
  57.2 6.1 %collective-permute-start.8 = (bf16[32,1536]{1,0:T(8,128)(2,1)S(1)}, bf16[32,1536]{1,0:T(8,128)(2,1)S(1)}, u32[]{:S(2)}, u32[]{:S(2)}) collective-permute-start(bf16[32,1536]{1,0:T(8,128)(2,1)S(1)} %pad_maximum_fusion.3), channel_id=1, source_target_pairs={{0,8},{8,16},{16,24},{24,0},{1,9},{9,17},{17,25},{25,1},{2,10},{10... | collective-permute-start | bytes 294920 | tf_op jit(solution)/shard_map/ppermute | solution.py:36
  57.2 6.1 %collective-permute-start.9 = (bf16[32,1536]{1,0:T(8,128)(2,1)S(1)}, bf16[32,1536]{1,0:T(8,128)(2,1)S(1)}, u32[]{:S(2)}, u32[]{:S(2)}) collective-permute-start(bf16[32,1536]{1,0:T(8,128)(2,1)S(1)} %pad_maximum_fusion.3), channel_id=1, source_target_pairs={{0,16},{8,24},{16,0},{24,8},{1,17},{9,25},{17,1},{25,9},{2,18},{10... | collective-permute-start | bytes 294920 | tf_op jit(solution)/shard_map/ppermute | solution.py:36
  76.1 21.8 %copy-start.9 = (f32[4]{0:T(128)S(1)}, f32[4]{0:T(128)}, u32[]{:S(2)}) copy-start(f32[4]{0:T(128)} %param.34) | copy-start | bytes 52
  76.1 27.1 %copy-start.8 = (f32[4]{0:T(128)S(1)}, f32[4]{0:T(128)}, u32[]{:S(2)}) copy-start(f32[4]{0:T(128)} %param.35) | copy-start | bytes 52
  76.1 14.6 %all-to-all-start.1 = ((bf16[8,32,512]{2,1,0:T(8,128)(2,1)}), bf16[8,32,512]{2,1,0:T(8,128)(2,1)S(1)}, u32[]{:S(2)}, u32[]{:S(2)}) async-start(bf16[8,32,512]{2,1,0:T(8,128)(2,1)} %broadcast_in_dim.86), calls=%async_computation.1 | async-start | bytes 524288 | tf_op jit(solution)/shard_map/all_to_all | solution.py:21
  84.3 19.2 %copy-start = (f32[8,4,128,128]{3,2,1,0:T(8,128)S(1)}, f32[8,4,128,128]{3,2,1,0:T(8,128)}, u32[]{:S(2)}) copy-start(f32[8,4,128,128]{3,2,1,0:T(8,128)} %param.22) | copy-start | bytes 6291460
  84.3 41.0 %all-gather.3.cloned.1.call-start = ((), (), s32[]{:S(2)}) async-start(), calls=%async_computation.6 | async-start | bytes 3096576 | tf_op jit(solution)/shard_map/all_gather | solution.py:160
  93.7 9.0 %all-to-all-start.2 = ((bf16[4,8,1664]{2,1,0:T(8,128)(2,1)}), bf16[4,8,1664]{2,1,0:T(8,128)(2,1)S(1)}, u32[]{:S(2)}, u32[]{:S(2)}) async-start(bf16[4,8,1664]{2,1,0:T(8,128)(2,1)} %pad_maximum_fusion.2), calls=%async_computation.2 | async-start | bytes 212992 | tf_op jit(solution)/shard_map/all_to_all | solution.py:21
  106.3 1.3 copy-start.1
  106.3 3.3 %copy-start.7 = (f32[128]{0:T(128)S(1)}, f32[128]{0:T(128)}, u32[]{:S(2)}) copy-start(f32[128]{0:T(128)} %param.36) | copy-start | bytes 1540
  142.4 4.9 %collective-permute-start.11 = (bf16[32,1536]{1,0:T(8,128)(2,1)S(1)}, bf16[32,1536]{1,0:T(8,128)(2,1)S(1)}, u32[]{:S(2)}, u32[]{:S(2)}) collective-permute-start(bf16[32,1536]{1,0:T(8,128)(2,1)S(1)} %pad_maximum_fusion.4), channel_id=1, source_target_pairs={{0,8},{8,16},{16,24},{24,0},{1,9},{9,17},{17,25},{25,1},{2,10},{10... | collective-permute-start | bytes 294920 | tf_op jit(solution)/shard_map/ppermute | solution.py:36
  143.7 6.2 %collective-permute-start.12 = (bf16[32,1536]{1,0:T(8,128)(2,1)S(1)}, bf16[32,1536]{1,0:T(8,128)(2,1)S(1)}, u32[]{:S(2)}, u32[]{:S(2)}) collective-permute-start(bf16[32,1536]{1,0:T(8,128)(2,1)S(1)} %pad_maximum_fusion.4), channel_id=1, source_target_pairs={{0,16},{8,24},{16,0},{24,8},{1,17},{9,25},{17,1},{25,9},{2,18},{10... | collective-permute-start | bytes 294920 | tf_op jit(solution)/shard_map/ppermute | solution.py:36
  146.3 4.5 %collective-permute-start.13 = (bf16[32,1536]{1,0:T(8,128)(2,1)S(1)}, bf16[32,1536]{1,0:T(8,128)(2,1)S(1)}, u32[]{:S(2)}, u32[]{:S(2)}) collective-permute-start(bf16[32,1536]{1,0:T(8,128)(2,1)S(1)} %pad_maximum_fusion.4), channel_id=1, source_target_pairs={{0,24},{8,0},{16,8},{24,16},{1,25},{9,1},{17,9},{25,17},{2,26},{10... | collective-permute-start | bytes 294920 | tf_op jit(solution)/shard_map/ppermute | solution.py:36
Sparse Core Ops, SparseCore 0:
  32.5 41.3 all-gather.4
  86.9 38.3 all-gather.2
